TPU v7x, 32 devices: a whole 2x2x4 slice. The times are simulated.
32 devices in a mesh: ep: 8 (over z, x), tp: 4 (over y, core).
Axes of the slice: x: 2, y: 2, z: 4, core: 2. Of those that a mesh axis runs over, the one named last changes fastest.
Arguments:
- tokens: bfloat16 [2048, 2048], P('ep'), may hold values from -40 to 40
- cotangent: bfloat16 [2048, 2048], P('ep'), may hold values from -6 to 6
- expert_ids: int32 [2048, 4], P('ep'), may hold values from 0 to 15, all different within a row; in each aligned block of 256 rows (0 to 255, 256 to 511, ...) at most 96 rows name the same one
- route_weights: bfloat16 [2048, 4], P('ep'), may hold values from 0.099609375 to 1
- gate_weight: bfloat16 [16, 2048, 2048], P('ep', None, 'tp'), may hold values from -0.125 to 0.125
- up_weight: bfloat16 [16, 2048, 2048], P('ep', None, 'tp'), may hold values from -0.125 to 0.125
- down_weight: bfloat16 [16, 2048, 2048], P('ep', 'tp'), may hold values from -0.125 to 0.125
- dense_weight: bfloat16 [2048, 2048], P('tp', 'ep'), may hold values from -0.125 to 0.125
- dense_gate: float32 [2048], replicated, may hold values from 0.1 to 1.9
Outputs:
- token_grad: bfloat16 [2048, 2048], P('ep', 'tp')
- weight_grad: bfloat16 [2048, 4], P('ep')
- gate_grad: float32 [16, 2048, 2048], P('ep', None, 'tp')
- up_grad: float32 [16, 2048, 2048], P('ep', None, 'tp')
- down_grad: float32 [16, 2048, 2048], P('ep', 'tp')
- dense_grad: float32 [2048, 2048], P('tp', 'ep')
Inputs may be any that keep to these rules, and one draw needn't show every extreme that they name: `expert_ids`: in the rows of one device, at most 96 routed rows name any one expert, and in every draw some expert is named by exactly 96 rows of some device.
All inputs are finite; a program needn't handle non-finite values.
Results may differ from a plain program's by a relative error of at most 0.02.
Values may be sent and summed in bfloat16 or wider, within the bound.
No kernel may reach another device: no remote copies, remote signals or barrier semaphores. Data moves between devices by JAX's collectives and lax.ppermute only.
A program may use at most 128 MiB of HBM per device.

v0:
```python
import jax
import jax.numpy as jnp
from jax import lax
from jax.sharding import PartitionSpec as P

clamp_limit = 7.0
sigmoid_slope = 1.702


def expert_back(row_input, row_cotan, row_weight, w_gate, w_up, w_down):
    gate_pre = jnp.dot(row_input, w_gate, preferred_element_type=jnp.float32)
    up_pre = jnp.dot(row_input, w_up, preferred_element_type=jnp.float32)
    gate_val = jnp.minimum(gate_pre, clamp_limit)
    up_val = jnp.clip(up_pre, -clamp_limit, clamp_limit)
    squash = jax.nn.sigmoid(sigmoid_slope * gate_val)
    hidden = ((up_val + 1.0) * gate_val * squash).astype(jnp.bfloat16)
    down_back = lax.dot_general(
        row_cotan, w_down, (((1,), (1,)), ((), ())), preferred_element_type=jnp.float32
    )
    scores = jnp.sum(hidden.astype(jnp.float32) * down_back, axis=1)
    scale_col = row_weight.astype(jnp.float32)[:, None]
    hidden_back = scale_col * down_back
    gate_slope = squash + sigmoid_slope * gate_val * squash * (1.0 - squash)
    gate_back = jnp.where(
        gate_pre < clamp_limit, hidden_back * (up_val + 1.0) * gate_slope, 0.0
    ).astype(jnp.bfloat16)
    up_back = jnp.where(jnp.abs(up_pre) < clamp_limit, hidden_back * gate_val * squash, 0.0).astype(
        jnp.bfloat16
    )
    weighted = (scale_col * row_cotan.astype(jnp.float32)).astype(jnp.bfloat16)
    input_back = lax.dot_general(
        gate_back, w_gate, (((1,), (1,)), ((), ())), preferred_element_type=jnp.float32
    )
    input_back = input_back + lax.dot_general(
        up_back, w_up, (((1,), (1,)), ((), ())), preferred_element_type=jnp.float32
    )
    grad_gate = lax.dot_general(
        row_input, gate_back, (((0,), (0,)), ((), ())), preferred_element_type=jnp.float32
    )
    grad_up = lax.dot_general(
        row_input, up_back, (((0,), (0,)), ((), ())), preferred_element_type=jnp.float32
    )
    grad_down = lax.dot_general(
        hidden, weighted, (((0,), (0,)), ((), ())), preferred_element_type=jnp.float32
    )
    return (input_back, scores, grad_gate, grad_up, grad_down)


def shards(
    tokens,
    cotangent,
    expert_ids,
    route_weights,
    gate_weight,
    up_weight,
    down_weight,
    dense_weight,
    dense_gate,
):
    tok_rows, model_width = tokens.shape
    top_count = expert_ids.shape[1]
    local_count = gate_weight.shape[0]
    ep_size = lax.axis_size("ep")
    tp_size = lax.axis_size("tp")
    expert_total = local_count * ep_size
    capacity = tok_rows * top_count * 3 // (2 * expert_total)
    routed = tok_rows * top_count
    feature_part = model_width // tp_size
    flat_ids = expert_ids.reshape(routed)
    onehot = (flat_ids[:, None] == jnp.arange(expert_total, dtype=jnp.int32)[None, :]).astype(
        jnp.int32
    )
    row_ranks = jnp.sum(onehot * (jnp.cumsum(onehot, axis=0) - 1), axis=1)
    slot_ids = flat_ids * capacity + row_ranks
    slot_rows = (
        jnp.full((expert_total * capacity,), routed, jnp.int32)
        .at[slot_ids]
        .set(jnp.arange(routed, dtype=jnp.int32))
    )
    slot_tokens = slot_rows // top_count
    zero_row = jnp.zeros((1, model_width), jnp.bfloat16)
    send_input = jnp.concatenate([tokens, zero_row], axis=0)[slot_tokens].reshape(
        ep_size, local_count * capacity, model_width
    )
    send_cotan = jnp.concatenate([cotangent, zero_row], axis=0)[slot_tokens].reshape(
        ep_size, local_count * capacity, model_width
    )
    send_weight = jnp.concatenate([route_weights.reshape(routed), jnp.zeros((1,), jnp.bfloat16)])[
        slot_rows
    ]
    send_weight = send_weight.reshape(ep_size, local_count * capacity)
    feature_start = lax.axis_index("tp") * feature_part
    cut_input = lax.dynamic_slice_in_dim(send_input, feature_start, feature_part, 2)
    cut_cotan = lax.dynamic_slice_in_dim(send_cotan, feature_start, feature_part, 2)
    part_input, part_cotan, recv_weight = (
        lax.all_to_all(cut_input, "ep", split_axis=0, concat_axis=0, tiled=True),
        lax.all_to_all(cut_cotan, "ep", split_axis=0, concat_axis=0, tiled=True),
        lax.all_to_all(send_weight, "ep", split_axis=0, concat_axis=0, tiled=True),
    )
    recv_input, recv_cotan = (
        lax.all_gather(part_input, "tp", axis=2, tiled=True),
        lax.all_gather(part_cotan, "tp", axis=2, tiled=True),
    )
    input_backs, score_list, gate_list, up_list, down_list = ([], [], [], [], [])
    for local_index in range(local_count):
        low = local_index * capacity
        row_input = recv_input[:, low : low + capacity].reshape(ep_size * capacity, model_width)
        row_cotan = recv_cotan[:, low : low + capacity].reshape(ep_size * capacity, model_width)
        row_weight = recv_weight[:, low : low + capacity].reshape(ep_size * capacity)
        pieces_out = expert_back(
            row_input,
            row_cotan,
            row_weight,
            gate_weight[local_index],
            up_weight[local_index],
            down_weight[local_index],
        )
        input_backs.append(pieces_out[0])
        score_list.append(pieces_out[1])
        gate_list.append(pieces_out[2])
        up_list.append(pieces_out[3])
        down_list.append(pieces_out[4])
    back_terms = jnp.stack(input_backs)
    score_cols = jnp.broadcast_to(
        jnp.stack(score_list)[:, :, None], (local_count, ep_size * capacity, tp_size)
    )
    summed, score_sum = (
        lax.psum_scatter(
            back_terms.astype(jnp.bfloat16), "tp", scatter_dimension=2, tiled=True
        ).astype(jnp.float32),
        lax.psum_scatter(
            score_cols.astype(jnp.bfloat16), "tp", scatter_dimension=2, tiled=True
        ).astype(jnp.float32),
    )
    back_rows = summed.astype(jnp.bfloat16).reshape(local_count, ep_size, capacity, feature_part)
    back_rows = back_rows.transpose(1, 0, 2, 3).reshape(
        ep_size, local_count * capacity, feature_part
    )
    back_score = score_sum[:, :, 0].astype(jnp.bfloat16).reshape(local_count, ep_size, capacity)
    back_score = back_score.transpose(1, 0, 2).reshape(ep_size, local_count * capacity)
    got_rows, got_score = (
        lax.all_to_all(back_rows, "ep", split_axis=0, concat_axis=0, tiled=True),
        lax.all_to_all(back_score, "ep", split_axis=0, concat_axis=0, tiled=True),
    )
    row_back = got_rows.reshape(expert_total * capacity, feature_part)[slot_ids]
    score_rows = got_score.reshape(expert_total * capacity)[slot_ids]
    gated_cotan = (dense_gate[None, :] * cotangent.astype(jnp.float32)).astype(jnp.bfloat16)
    columns = gated_cotan
    dense_back = lax.dot_general(
        columns,
        lax.all_gather(dense_weight, "ep", axis=1, tiled=True),
        (((1,), (1,)), ((), ())),
        preferred_element_type=jnp.float32,
    )
    own_input = lax.dynamic_slice_in_dim(
        tokens, lax.axis_index("tp") * feature_part, feature_part, 1
    )
    columns = gated_cotan
    dense_share = lax.psum_scatter(
        lax.dot_general(
            columns, own_input, (((0,), (0,)), ((), ())), preferred_element_type=jnp.float32
        ).astype(jnp.bfloat16),
        "ep",
        scatter_dimension=0,
        tiled=True,
    ).astype(jnp.float32)
    dense_grad = dense_share.T
    token_grad = (
        jnp.sum(row_back.reshape(tok_rows, top_count, feature_part).astype(jnp.float32), axis=1)
        + dense_back
    ).astype(jnp.bfloat16)
    weight_grad = score_rows.reshape(tok_rows, top_count)
    return (
        token_grad,
        weight_grad,
        jnp.stack(gate_list),
        jnp.stack(up_list),
        jnp.stack(down_list),
        dense_grad,
    )


def solution(mesh):
    in_specs = (
        P("ep", None),
        P("ep", None),
        P("ep", None),
        P("ep", None),
        P("ep", None, "tp"),
        P("ep", None, "tp"),
        P("ep", "tp", None),
        P("tp", "ep"),
        P(),
    )
    out_specs = (
        P("ep", "tp"),
        P("ep", None),
        P("ep", None, "tp"),
        P("ep", None, "tp"),
        P("ep", "tp", None),
        P("tp", "ep"),
    )
    return jax.shard_map(shards, mesh=mesh, in_specs=in_specs, out_specs=out_specs, check_vma=False)
```

profile of v0, /device:TPU:0, one launch (start us, length us, event | category | flops | bytes accessed | tf_op | source)
XLA Modules:
  0.0 354.2 jit_solution(9890774017876593381)
XLA Ops:
  10.1 4.5 %reduce-window.6 = s32[16,8,128]{2,1,0:T(8,128)S(1)} reduce-window(s32[16,8,128]{2,1,0:T(8,128)S(1)} %fusion.36, s32[]{:T(128)} %constant.13.clone.1), window={size=1x1x128 pad=0_0x0_0x127_0}, to_apply=%region_0.0 | reduce-window | flops 2080768 | bytes 131076 | tf_op jit(solution)/shard_map/reduce-window
  15.1 4.3 %scatter_custom_fusion = s32[1536]{0:T(1024)S(1)} fusion(s32[1024]{0:T(1024)S(1)} %bitcast.123, s32[1024]{0:T(1024)S(1)} %iota.11, s32[]{:T(128)} %constant.21.clone.1), kind=kCustom, calls=%fused_computation.93 | custom fusion | bytes 6148 | tf_op jit(solution)/shard_map/scatter | solution.py:78
  20.8 7.0 %gather_fusion = bf16[1536,2048]{1,0:T(8,128)(2,1)} fusion(bf16[257,2048]{1,0:T(8,128)(2,1)S(1)} %concatenate.9, s32[2048]{0:T(1024)S(1)} %get-tuple-element.45), kind=kCustom, calls=%fused_computation | custom fusion | bytes 12589056 | tf_op jit(solution)/shard_map/gather | solution.py:82
  29.2 44.3 %all_to_all.38 = bf16[8,192,512]{2,1,0:T(8,128)(2,1)} all-to-all(bf16[8,192,512]{2,1,0:T(8,128)(2,1)S(1)} %constant_dynamic-slice_fusion.1), channel_id=1, replica_groups=mesh['ep'=8,'tp'=4] {'ep'}, dimensions={0} | all-to-all | bytes 3145728 | tf_op jit(solution)/shard_map/all_to_all | solution.py:96
  73.8 7.0 %gather_fusion.2 = bf16[1536,2048]{1,0:T(8,128)(2,1)} fusion(bf16[257,2048]{1,0:T(8,128)(2,1)S(1)} %concatenate.11, s32[2048]{0:T(1024)S(1)} %get-tuple-element.45), kind=kCustom, calls=%fused_computation.2 | custom fusion | bytes 12589056 | tf_op jit(solution)/shard_map/gather | solution.py:85
  82.5 40.2 %all_to_all.39 = bf16[8,192,512]{2,1,0:T(8,128)(2,1)} all-to-all(bf16[8,192,512]{2,1,0:T(8,128)(2,1)S(1)} %constant_dynamic-slice_fusion), channel_id=1, replica_groups=mesh['ep'=8,'tp'=4] {'ep'}, dimensions={0} | all-to-all | bytes 3145728 | tf_op jit(solution)/shard_map/all_to_all | solution.py:97
  123.0 9.5 %gather_fusion.1 = bf16[1536]{0:T(1024)(128)(2,1)S(1)} fusion(bf16[1025]{0:T(1024)(128)(2,1)S(1)} %pad_maximum_fusion.4, s32[2048]{0:T(1024)S(1)} %get-tuple-element.44), kind=kCustom, calls=%fused_computation.1 | custom fusion | bytes 12288 | tf_op jit(solution)/shard_map/gather | solution.py:88
  155.0 13.2 %all-gather.6.cloned.1.call-done = bf16[8,192,2048]{2,1,0:T(8,128)(2,1)} async-done(((bf16[8,192,512]{2,1,0:T(8,128)(2,1)}), bf16[8,192,2048]{2,1,0:T(8,128)(2,1)}) %all-gather.6.cloned.1.call-update) | async-done | bytes 6291472 | tf_op jit(solution)/shard_map/all_gather | solution.py:102
  174.4 3.9 %multiply_reduce_fusion = (bf16[768]{0:T(1024)(128)(2,1)S(1)}, bf16[768,512]{0,1:T(8,128)(2,1)}, bf16[768,512]{0,1:T(8,128)(2,1)S(1)}, bf16[768,512]{0,1:T(8,128)(2,1)S(1)}) fusion(f32[768,512]{0,1:T(8,128)S(1)} %copy-done.25, f32[768,512]{0,1:T(8,128)S(1)} %copy-done.26, f32[768]{0:T(1024)S(1)} %reshape.143, bf16[768,2048]{1,0:T(8,128)(2,1)S(1)} %bitcast.112, ...), kind=kOutput, calls=%fused_computation.54 | convolution fusion | flops 1622015232 | bytes 10753536 | tf_op jit(solution)/shard_map/dot_general | solution.py:17
  184.5 3.9 %multiply_reduce_fusion.1 = (bf16[768]{0:T(1024)(128)(2,1)S(1)}, bf16[768,512]{0,1:T(8,128)(2,1)}, bf16[768,512]{0,1:T(8,128)(2,1)S(1)}, bf16[768,512]{0,1:T(8,128)(2,1)S(1)}) fusion(f32[768,512]{0,1:T(8,128)S(1)} %fusion.20, f32[768,512]{0,1:T(8,128)S(1)} %fusion.14, f32[768]{0:T(1024)S(1)} %reshape.142, bf16[768,2048]{1,0:T(8,128)(2,1)S(1)} %bitcast.106, ...), kind=kOutput, calls=%fused_computation.56 | convolution fusion | flops 1622015232 | bytes 10753536 | tf_op jit(solution)/shard_map/dot_general | solution.py:17
  198.5 12.4 %reduce-scatter.5.cloned.1.call-done = bf16[256,512]{1,0:T(8,128)(2,1)} async-done(((bf16[2048,512]{1,0:T(8,128)(2,1)}), bf16[256,512]{1,0:T(8,128)(2,1)}) %reduce-scatter.5.cloned.1.call-update) | async-done | bytes 262160 | tf_op jit(solution)/shard_map/reduce_scatter | solution.py:159
  214.8 5.9 %convolution_bitcast_fusion.4 = f32[1,2048,512]{2,1,0:T(8,128)} fusion(bf16[768,2048]{1,0:T(8,128)(2,1)} %bitcast.116, bf16[768,512]{0,1:T(8,128)(2,1)} %copy-done.18), kind=kOutput, calls=%fused_computation.18 | convolution fusion | flops 1610612736 | bytes 8126464 | tf_op jit(solution)/shard_map/dot_general | solution.py:37
  220.8 10.1 %all-reduce.2 = bf16[2,768,4]{1,0,2:T(2,128)(2,1)S(1)} all-reduce(bf16[2,768,4]{1,0,2:T(2,128)(2,1)S(1)} %broadcast_in_dim.35), channel_id=3, replica_groups=mesh['ep'=8,'tp'=4] {'tp'}, use_global_device_ids=true, to_apply=%region_8.9.clone | all-reduce | flops 6144 | bytes 24576
  232.3 3.9 %all-to-all-start.4 = ((bf16[8,1,192]{2,1,0:T(2,128)(2,1)}), bf16[8,1,192]{2,1,0:T(2,128)(2,1)S(1)}, u32[]{:S(2)}, u32[]{:S(2)}) async-start(bf16[8,1,192]{2,1,0:T(2,128)(2,1)} %all_to_all.32), calls=%async_computation.5 | async-start | bytes 16384 | tf_op jit(solution)/shard_map/all_to_all | solution.py:143
  236.3 4.9 %convolution_bitcast_fusion.5 = f32[1,2048,512]{2,1,0:T(8,128)} fusion(bf16[768,2048]{1,0:T(8,128)(2,1)S(1)} %bitcast.110, bf16[768,512]{0,1:T(8,128)(2,1)} %copy-done.17), kind=kOutput, calls=%fused_computation.19 | convolution fusion | flops 1610612736 | bytes 8126464 | tf_op jit(solution)/shard_map/dot_general | solution.py:37
  241.2 29.3 %reduce-scatter.3.cloned.1.call-done = bf16[2,768,512]{2,1,0:T(8,128)(2,1)} async-done(((bf16[2,768,2048]{2,1,0:T(8,128)(2,1)}), bf16[2,768,512]{2,1,0:T(8,128)(2,1)}) %reduce-scatter.3.cloned.1.call-update) | async-done | bytes 1572880 | tf_op jit(solution)/shard_map/reduce_scatter | solution.py:128
  273.2 5.7 %all-to-all-start.3 = ((bf16[8,192,512]{2,1,0:T(8,128)(2,1)}), bf16[8,192,512]{2,1,0:T(8,128)(2,1)S(1)}, u32[]{:S(2)}, u32[]{:S(2)}) async-start(bf16[8,192,512]{2,1,0:T(8,128)(2,1)} %bitcast.20), calls=%async_computation.4 | async-start | bytes 3145728 | tf_op jit(solution)/shard_map/all_to_all | solution.py:142
  279.0 8.2 %pad_maximum_fusion = f32[2,2048,512]{2,1,0:T(8,128)} fusion(f32[1,2048,512]{2,1,0:T(8,128)} %convolution_bitcast_fusion.4, f32[1,2048,512]{2,1,0:T(8,128)} %convolution_bitcast_fusion.5), kind=kLoop, calls=%fused_computation.6 | loop fusion | flops 2097152 | bytes 16777216 | tf_op jit(solution)/shard_map/stack | solution.py:176
  291.2 4.4 %pad_maximum_fusion.1 = f32[2,2048,512]{2,1,0:T(8,128)} fusion(f32[1,2048,512]{2,1,0:T(8,128)S(1)} %convolution_bitcast_fusion.2, f32[1,2048,512]{2,1,0:T(8,128)S(1)} %convolution_bitcast_fusion.3), kind=kLoop, calls=%fused_computation.7 | loop fusion | flops 2097152 | bytes 16777216 | tf_op jit(solution)/shard_map/stack | solution.py:177
  299.6 4.0 %pad_maximum_fusion.2 = f32[2,512,2048]{2,1,0:T(8,128)} fusion(f32[1,512,2048]{2,1,0:T(8,128)S(1)} %convolution_bitcast_fusion, f32[1,512,2048]{2,1,0:T(8,128)S(1)} %convolution_bitcast_fusion.1), kind=kLoop, calls=%fused_computation.8 | loop fusion | flops 2097152 | bytes 16777216 | tf_op jit(solution)/shard_map/stack | solution.py:178
  303.7 6.8 %gather_fusion.4 = bf16[1024]{0:T(1024)(128)(2,1)S(1)} fusion(bf16[1536]{0:T(1024)(128)(2,1)S(1)} %reshape.140, s32[1024]{0:T(1024)S(1)} %broadcast_clamp_fusion), kind=kCustom, calls=%fused_computation.4 | custom fusion | bytes 8192 | tf_op jit(solution)/shard_map/gather | solution.py:146
  311.4 16.8 %all-to-all-done.3 = bf16[8,192,512]{2,1,0:T(8,128)(2,1)S(1)} async-done(((bf16[8,192,512]{2,1,0:T(8,128)(2,1)}), bf16[8,192,512]{2,1,0:T(8,128)(2,1)S(1)}, u32[]{:S(2)}, u32[]{:S(2)}) %all-to-all-start.3) | async-done | bytes 1572896 | tf_op jit(solution)/shard_map/all_to_all | solution.py:142
  328.1 4.0 %gather_fusion.3 = bf16[1024,512]{1,0:T(8,128)(2,1)S(1)} fusion(bf16[1536,512]{1,0:T(8,128)(2,1)S(1)} %bitcast.103, s32[1024]{0:T(1024)S(1)} %broadcast_clamp_fusion), kind=kCustom, calls=%fused_computation.3 | custom fusion | bytes 2101248 | tf_op jit(solution)/shard_map/gather | solution.py:145
  334.1 8.9 %all-gather.8.cloned.1.call-done = bf16[512,2048]{1,0:T(8,128)(2,1)} async-done(((bf16[512,256]{1,0:T(8,128)(2,1)}), bf16[512,2048]{1,0:T(8,128)(2,1)}) %all-gather.8.cloned.1.call-update) | async-done | bytes 2097168 | tf_op jit(solution)/shard_map/all_gather | solution.py:151
  (134 shorter events, 74.6 us)
Async XLA Ops:
  8.0 135.4 %all-gather.4.cloned.1.call-start = ((), (), s32[]{:S(2)}) async-start(), calls=%async_computation.7 | async-start | bytes 7864320 | tf_op jit(solution)/shard_map/all_gather | solution.py:101
  29.2 44.4 %copy-start = (bf16[256,2048]{1,0:T(8,128)(2,1)S(1)}, bf16[256,2048]{1,0:T(8,128)(2,1)}, u32[]{:S(2)}) copy-start(bf16[256,2048]{1,0:T(8,128)(2,1)} %param.10) | copy-start | bytes 3145732
  73.6 94.6 %all-gather.6.cloned.1.call-start = ((), (), s32[]{:S(2)}) async-start(), calls=%async_computation.8 | async-start | bytes 7864320 | tf_op jit(solution)/shard_map/all_gather | solution.py:102
  82.5 40.2 %copy-start.20 = (bf16[256,4]{0,1:T(4,128)(2,1)S(1)}, bf16[256,4]{0,1:T(4,128)(2,1)}, u32[]{:S(2)}) copy-start(bf16[256,4]{0,1:T(4,128)(2,1)} %param.12) | copy-start | bytes 6148
  122.6 14.1 %copy-start.19 = (f32[2048]{0:T(1024)S(1)}, f32[2048]{0:T(1024)}, u32[]{:S(2)}) copy-start(f32[2048]{0:T(1024)} %param.17) | copy-start | bytes 24580
  133.1 10.1 %all-to-all-start.1 = ((bf16[8,1,192]{2,1,0:T(2,128)(2,1)}), bf16[8,1,192]{2,1,0:T(2,128)(2,1)S(1)}, u32[]{:S(2)}, u32[]{:S(2)}) async-start(bf16[8,1,192]{2,1,0:T(2,128)(2,1)} %all_to_all.31), calls=%async_computation.1 | async-start | bytes 16384 | tf_op jit(solution)/shard_map/all_to_all | solution.py:98
  136.6 74.3 %reduce-scatter.5.cloned.1.call-start = ((), (), s32[]{:S(2)}) async-start(), calls=%async_computation.11 | async-start | bytes 2359296 | tf_op jit(solution)/shard_map/reduce_scatter | solution.py:159
  139.8 130.8 %reduce-scatter.3.cloned.1.call-start = ((), (), s32[]{:S(2)}) async-start(), calls=%async_computation.9 | async-start | bytes 7864320 | tf_op jit(solution)/shard_map/reduce_scatter | solution.py:128
  143.4 4.1 %copy-start.1 = (bf16[2,2048,512]{2,1,0:T(8,128)(2,1)S(1)}, bf16[2,2048,512]{2,1,0:T(8,128)(2,1)}, u32[]{:S(2)}) copy-start(bf16[2,2048,512]{2,1,0:T(8,128)(2,1)} %param.13) | copy-start | bytes 12582916
  147.0 89.3 %copy-start.7 = (bf16[8,96,2048]{2,1,0:T(8,128)(2,1)}, bf16[8,96,2048]{2,1,0:T(8,128)(2,1)S(1)}, u32[]{:S(2)}) copy-start(bf16[8,96,2048]{2,1,0:T(8,128)(2,1)S(1)} %get-tuple-element.30) | copy-start | bytes 9437188
  147.5 4.5 %copy-start.3 = (bf16[2,2048,512]{2,1,0:T(8,128)(2,1)S(1)}, bf16[2,2048,512]{2,1,0:T(8,128)(2,1)}, u32[]{:S(2)}) copy-start(bf16[2,2048,512]{2,1,0:T(8,128)(2,1)} %param.14) | copy-start | bytes 12582916
  168.2 4.1 %copy-start.21 = (bf16[2,512,2048]{2,1,0:T(8,128)(2,1)S(1)}, bf16[2,512,2048]{2,1,0:T(8,128)(2,1)}, u32[]{:S(2)}) copy-start(bf16[2,512,2048]{2,1,0:T(8,128)(2,1)} %param.15) | copy-start | bytes 12582916
  168.2 4.6 %copy-start.25 = (f32[768,512]{0,1:T(8,128)S(1)}, f32[768,512]{0,1:T(8,128)}, u32[]{:S(2)}) copy-start(f32[768,512]{0,1:T(8,128)} %fusion.11) | copy-start | bytes 4718596
  168.2 6.3 %copy-start.26 = (f32[768,512]{0,1:T(8,128)S(1)}, f32[768,512]{0,1:T(8,128)}, u32[]{:S(2)}) copy-start(f32[768,512]{0,1:T(8,128)} %fusion.5) | copy-start | bytes 4718596
  171.8 6.5 %copy-start.9 = (bf16[8,96,2048]{2,1,0:T(8,128)(2,1)}, bf16[8,96,2048]{2,1,0:T(8,128)(2,1)S(1)}, u32[]{:S(2)}) copy-start(bf16[8,96,2048]{2,1,0:T(8,128)(2,1)S(1)} %get-tuple-element.29) | copy-start | bytes 9437188
  171.8 12.7 %copy-start.5 = (bf16[8,96,2048]{2,1,0:T(8,128)(2,1)}, bf16[8,96,2048]{2,1,0:T(8,128)(2,1)S(1)}, u32[]{:S(2)}) copy-start(bf16[8,96,2048]{2,1,0:T(8,128)(2,1)S(1)} %get-tuple-element.28) | copy-start | bytes 9437188
  178.3 12.0 %copy-start.13 = (bf16[768,512]{0,1:T(8,128)(2,1)}, bf16[768,512]{0,1:T(8,128)(2,1)S(1)}, u32[]{:S(2)}) copy-start(bf16[768,512]{0,1:T(8,128)(2,1)S(1)} %get-tuple-element.39) | copy-start | bytes 2359300
  197.3 145.7 %all-gather.8.cloned.1.call-start = ((), (), s32[]{:S(2)}) async-start(), calls=%async_computation.10 | async-start | bytes 2359296 | tf_op jit(solution)/shard_map/all_gather | solution.py:151
  232.3 40.9 %all-to-all-start.4 = ((bf16[8,1,192]{2,1,0:T(2,128)(2,1)}), bf16[8,1,192]{2,1,0:T(2,128)(2,1)S(1)}, u32[]{:S(2)}, u32[]{:S(2)}) async-start(bf16[8,1,192]{2,1,0:T(2,128)(2,1)} %all_to_all.32), calls=%async_computation.5 | async-start | bytes 16384 | tf_op jit(solution)/shard_map/all_to_all | solution.py:143
  273.2 54.9 %all-to-all-start.3 = ((bf16[8,192,512]{2,1,0:T(8,128)(2,1)}), bf16[8,192,512]{2,1,0:T(8,128)(2,1)S(1)}, u32[]{:S(2)}, u32[]{:S(2)}) async-start(bf16[8,192,512]{2,1,0:T(8,128)(2,1)} %bitcast.20), calls=%async_computation.4 | async-start | bytes 3145728 | tf_op jit(solution)/shard_map/all_to_all | solution.py:142
  279.0 8.2 %copy-start.12 = (bf16[8,96,2048]{2,1,0:T(8,128)(2,1)S(1)}, bf16[8,96,2048]{2,1,0:T(8,128)(2,1)}, u32[]{:S(2)}) copy-start(bf16[8,96,2048]{2,1,0:T(8,128)(2,1)} %copy-done.11) | copy-start | bytes 9437188
  279.0 8.2 %copy-start.14 = (bf16[768,512]{0,1:T(8,128)(2,1)S(1)}, bf16[768,512]{0,1:T(8,128)(2,1)}, u32[]{:S(2)}) copy-start(bf16[768,512]{0,1:T(8,128)(2,1)} %copy-done.13) | copy-start | bytes 2359300
  291.2 4.4 %copy-start.10 = (bf16[8,96,2048]{2,1,0:T(8,128)(2,1)S(1)}, bf16[8,96,2048]{2,1,0:T(8,128)(2,1)}, u32[]{:S(2)}) copy-start(bf16[8,96,2048]{2,1,0:T(8,128)(2,1)} %copy-done.9) | copy-start | bytes 9437188
  291.2 4.4 %copy-start.23 = (bf16[768,512]{0,1:T(8,128)(2,1)S(1)}, bf16[768,512]{0,1:T(8,128)(2,1)}, u32[]{:S(2)}) copy-start(bf16[768,512]{0,1:T(8,128)(2,1)} %get-tuple-element.27) | copy-start | bytes 2359300
  (11 other events, 25.7 us)
Sparse Core Ops, SparseCore 0:
  73.7 45.3 all-gather.3
  122.8 45.3 all-gather.5
Sparse Core Ops, SparseCore 1:
  141.2 69.6 reduce-scatter.4
  213.9 56.6 reduce-scatter.2
  272.5 70.5 all-gather.7
where the time goes:
time: 360 us; the launch traced here: 354 us
  blocking collectives  94.6 us (26%)
  waiting for transfers between devices  84.1 us (23%)
  local copies, waits for them, and re-layouts  66.8 us (19%)
  matrix products  49.9 us (14%)
  other arithmetic  28.4 us (8%)
  between operations  16.4 us (5%)
  starting transfers between devices  13.9 us (4%)
    all_to_all x1, blocking collectives, shards(): lax.all_to_all(cut_input, 'ep', split_axis=0, concat_axis=0, tiled=True)  44.3 us
    all_to_all x1, blocking collectives, shards(): lax.all_to_all(cut_cotan, 'ep', split_axis=0, concat_axis=0, tiled=True)  40.2 us
    reduce_scatter x1, waiting for transfers between devices, shards(): lax.psum_scatter(back_terms.astype(jnp.bfloat16), 'tp', scatter_dimension...  29.3 us
    all_to_all x1, waiting for transfers between devices, shards(): lax.all_to_all(back_rows, 'ep', split_axis=0, concat_axis=0, tiled=True)  16.8 us
    all_gather x1, waiting for transfers between devices, shards(): lax.all_gather(part_cotan, 'tp', axis=2, tiled=True)  13.2 us
    reduce_scatter x1, waiting for transfers between devices, shards(): lax.psum_scatter(lax.dot_general(columns, own_input, (((0,), (0,)), ((),...  12.4 us
    dot_general x2, matrix products, expert_back(): lax.dot_general(row_input, gate_back, (((0,), (0,)), ((), ())), preferred...  10.9 us
    unnamed x61, local copies, waits for them, and re-layouts  10.3 us
  transfers between devices with their start and end apart: 8, of which 6 were waited for; matrix products, arithmetic and copies ran while one was open for 32% of the time, Pallas kernels for 0%

commit v1 on v0

v1 whole, which is shorter than its diff:
```python
import functools

import jax
import jax.numpy as jnp
from jax import lax
from jax.experimental import pallas as pl
from jax.experimental.pallas import tpu as pltpu
from jax.sharding import PartitionSpec as P


clamp_limit = 7.0
sigmoid_slope = 1.702
f32, bf16 = jnp.float32, jnp.bfloat16


def swap(value, axis, mask):
    size = lax.axis_size(axis)
    return lax.ppermute(value, axis, [(i, i ^ mask) for i in range(size)])


def columns(lhs, rhs):
    return lax.dot_general(lhs, rhs, (((1,), (1,)), ((), ())), preferred_element_type=f32)


def outer(lhs, rhs):
    return lax.dot_general(lhs, rhs, (((0,), (0,)), ((), ())), preferred_element_type=f32)


def pair_kernel(layout, local, cap, *refs):
    count = len(layout)
    inputs, refs = refs[: sum(n for n, _ in layout)], refs[sum(n for n, _ in layout) :]
    stored, (dense_w_ref, dense_g_ref, dgrad_in) = refs[:3], refs[3:6]
    held, (weight_sems, block, meta, picks, rows_s, cots_s, back, dense, score_total, sems) = (
        refs[-13:-10], refs[-10:]
    )
    wg_ref, wu_ref, wd_ref = held
    row_ref, hid_ref, gb_ref, ub_ref, wt_ref, keep_ref, send_ref, dgrad_ref = refs[-21:-13]
    tp, ep, e = lax.axis_index("tp"), lax.axis_index("ep"), pl.program_id(0)
    tp_size = lax.axis_size("tp")
    tok_rows, width = block.shape[2:]

    def weight_copy(i, j):
        return pltpu.make_async_copy(stored[i].at[j], held[i].at[j], weight_sems.at[i, j])

    top = meta.shape[1] // 2
    step = min(512, width)

    def table(b, expert):
        values = meta[b].astype(f32)
        match = (values[:top] == expert.astype(f32)).astype(f32)
        return (
            match,
            jnp.sum(match, axis=0, keepdims=True),
            jnp.sum(match * values[top:], axis=0, keepdims=True),
        )

    @pl.when(e == 0)
    def _():
        copies, counts, n = [], [0], 0

        def fetch(source, target):
            copy = pltpu.make_async_copy(source, target, sems.at[len(copies)])
            copy.start()
            copies.append(copy)

        for b, (number, masks) in enumerate(layout):
            mine = inputs[n : n + number]
            n += number
            if masks is None:
                fetch(mine[0], block.at[b, 0])
                fetch(mine[1], block.at[b, 1])
                fetch(mine[2], meta.at[b])
                counts.append(len(copies))
                continue
            for i, (piece, mask) in enumerate(zip(mine, masks)):
                rows = (piece.shape[0] - 2 * top) // 2
                other = tp ^ mask
                if rows * 2 == tok_rows:
                    place = (other % 2) * rows
                else:
                    place = ((other % 2) * (tp_size // 2) + other // 2) * rows
                place = pl.ds(pl.multiple_of(place, 16), rows)
                fetch(piece.at[:rows], block.at[b, 0, place])
                fetch(piece.at[rows : 2 * rows], block.at[b, 1, place])
                if i == 0:
                    fetch(piece.at[2 * rows :, :tok_rows], meta.at[b])
            counts.append(len(copies))
        for j in range(local):
            for i in range(3):
                weight_copy(i, j).start()
        before = (
            lax.broadcasted_iota(jnp.int32, (tok_rows, tok_rows), 0)
            < lax.broadcasted_iota(jnp.int32, (tok_rows, tok_rows), 1)
        )
        before = jnp.where(before, 1.0, 0.0).astype(bf16)
        slot = lax.broadcasted_iota(jnp.int32, (cap, tok_rows), 0).astype(f32)
        out_part, in_part = dense_w_ref.shape[1], dense_w_ref.shape[0]
        own_cols = pl.ds(pl.multiple_of(tp * in_part, 128), in_part)
        out_cols = pl.ds(pl.multiple_of(ep * out_part, 128), out_part)
        dense_sum = dgrad_in[...]
        for b in range(count):
            for copy in copies[counts[b] : counts[b + 1]]:
                copy.wait()
            for j in range(local):
                chosen = table(b, ep * local + j)[1]
                rank = jnp.dot(
                    jnp.broadcast_to(chosen, (8, tok_rows)).astype(bf16),
                    before,
                    preferred_element_type=f32,
                )[:1]
                place = jnp.where(chosen > 0.0, rank, -1.0)
                picks[b, j * cap : (j + 1) * cap] = jnp.where(slot == place, 1.0, 0.0).astype(bf16)
            for which, out in ((0, rows_s), (1, cots_s)):
                for low in range(0, width, step):
                    got = jnp.dot(
                        picks[b], block[b, which, :, low : low + step],
                        preferred_element_type=f32,
                    ).astype(bf16)
                    for j in range(local):
                        out[j, b * cap : (b + 1) * cap, low : low + step] = got[
                            j * cap : (j + 1) * cap
                        ]
            gated = (dense_g_ref[:, out_cols] * block[b, 1, :, out_cols].astype(f32)).astype(bf16)
            dense[b] = columns(gated, dense_w_ref[...])
            dense_sum = dense_sum + outer(block[b, 0, :, own_cols], gated)
        dgrad_ref[...] = dense_sum
        score_total[...] = jnp.zeros_like(score_total)

    for i in range(3):
        weight_copy(i, e).wait()
    rows, cots = rows_s[e], cots_s[e]
    row_ref[0] = rows
    own_rows = pl.ds(pl.multiple_of(e * cap, 16), cap)
    own_picks = [picks[b, own_rows] for b in range(count)]
    tables = [table(b, ep * local + e) for b in range(count)]
    scale = jnp.concatenate(
        [
            jnp.sum(own_picks[b].astype(f32) * tables[b][2], axis=1, keepdims=True)
            for b in range(count)
        ],
        axis=0,
    )
    gate_pre = jnp.dot(rows, wg_ref[e], preferred_element_type=f32)
    up_pre = jnp.dot(rows, wu_ref[e], preferred_element_type=f32)
    down_back = columns(cots, wd_ref[e])
    gate_val = jnp.minimum(gate_pre, clamp_limit)
    up_val = jnp.clip(up_pre, -clamp_limit, clamp_limit)
    squash = jax.nn.sigmoid(sigmoid_slope * gate_val)
    hidden = ((up_val + 1.0) * gate_val * squash).astype(bf16)
    product = hidden.astype(f32) * down_back
    hidden_back = scale * down_back
    gate_slope = squash + sigmoid_slope * gate_val * squash * (1.0 - squash)
    gate_back = jnp.where(
        gate_pre < clamp_limit, hidden_back * (up_val + 1.0) * gate_slope, 0.0
    ).astype(bf16)
    up_back = jnp.where(
        jnp.abs(up_pre) < clamp_limit, hidden_back * gate_val * squash, 0.0
    ).astype(bf16)
    hid_ref[0], gb_ref[0], ub_ref[0] = hidden, gate_back, up_back
    wt_ref[0] = (scale * cots.astype(f32)).astype(bf16)
    for low in range(0, width, step):
        cols = slice(low, low + step)
        value = (
            columns(gate_back, wg_ref[e, cols]) + columns(up_back, wu_ref[e, cols])
        ).astype(bf16)
        for b in range(count):
            back[b, own_rows, cols] = value[b * cap : (b + 1) * cap]
    score = jnp.sum(product, axis=1, keepdims=True)
    for b in range(count):
        by_token = jnp.sum(
            own_picks[b].astype(f32) * score[b * cap : (b + 1) * cap], axis=0, keepdims=True
        )
        score_total[b, :top] += tables[b][0] * by_token

    @pl.when(e == local - 1)
    def _():
        part = dense.shape[2]
        for b in range(count):
            for p in range(tp_size):
                out = send_ref if p % 2 else keep_ref
                cols = pl.ds(pl.multiple_of((tp ^ p) * part, 128), part)
                value = outer(picks[b], back[b, :, cols])
                if p == 0:
                    value = value + dense[b]
                out[b, p // 2, :tok_rows] = value.astype(bf16)
                out[b, p // 2, tok_rows:] = jnp.zeros((out.shape[2] - tok_rows, part), bf16)
                out[b, p // 2, tok_rows:, :tok_rows] = score_total[b].astype(bf16)


def expert_pair(
    blocks, weights, dense_w, dense_g, dgrad, slabs, index, count_all, tok_rows, cap, top
):
    local, width, units = weights[0].shape
    count = len(blocks)
    part = dense_w.shape[0]
    halves = lax.axis_size("tp") // 2
    m = count * cap
    vmem = pl.BlockSpec(memory_space=pltpu.VMEM)
    hbm = pl.BlockSpec(memory_space=pltpu.HBM)
    arrays = [v for values, _ in blocks for v in values]
    layout = tuple((len(values), masks) for values, masks in blocks)
    payload = jax.ShapeDtypeStruct((count, halves, tok_rows + 8, part), bf16)
    window = lambda lanes: pl.BlockSpec((1, m, lanes), lambda e: (e, index, 0))
    slab_lanes = (width, units, units, units, width)
    operands = [*arrays, *weights, dense_w, dense_g, dgrad]
    specs = [hbm] * (len(arrays) + 3) + [vmem] * 3
    aliases = {}
    if slabs is not None:
        aliases = {len(operands) + i: i for i in range(5)}
        operands += list(slabs)
        specs += [hbm] * 5
    return pl.pallas_call(
        functools.partial(pair_kernel, layout, local, cap),
        grid=(local,),
        out_shape=(
            *[jax.ShapeDtypeStruct((local, count_all * m, n), bf16) for n in slab_lanes],
            payload,
            payload,
            jax.ShapeDtypeStruct(dgrad.shape, f32),
        ),
        in_specs=specs,
        out_specs=(*[window(n) for n in slab_lanes], vmem, vmem, vmem),
        scratch_shapes=[
            *[pltpu.VMEM(w.shape, bf16) for w in weights],
            pltpu.SemaphoreType.DMA((3, local)),
            pltpu.VMEM((count, 2, tok_rows, width), bf16),
            pltpu.VMEM((count, 2 * top, tok_rows), bf16),
            pltpu.VMEM((count, local * cap, tok_rows), bf16),
            pltpu.VMEM((local, m, width), bf16),
            pltpu.VMEM((local, m, width), bf16),
            pltpu.VMEM((count, local * cap, width), bf16),
            pltpu.VMEM((count, tok_rows, part), f32),
            pltpu.VMEM((count, 8, tok_rows), f32),
            pltpu.SemaphoreType.DMA((3 * len(arrays),)),
        ],
        input_output_aliases=aliases,
        compiler_params=pltpu.CompilerParams(vmem_limit_bytes=56 << 20),
        cost_estimate=pl.CostEstimate(
            flops=14 * local * m * width * units,
            bytes_accessed=10 * local * width * units,
            transcendentals=local * m * units,
        ),
        name="expert_pair",
    )(*operands)


def batched(lhs, rhs):
    return lax.dot_general(lhs, rhs, (((1,), (1,)), ((0,), (0,))), preferred_element_type=f32)


def shards(
    tokens,
    cotangent,
    expert_ids,
    route_weights,
    gate_weight,
    up_weight,
    down_weight,
    dense_weight,
    dense_gate,
):
    tok_rows, width = tokens.shape
    top_count = expert_ids.shape[1]
    local = gate_weight.shape[0]
    ep_size = lax.axis_size("ep")
    tp_size = lax.axis_size("tp")
    ep, tp = lax.axis_index("ep"), lax.axis_index("tp")
    cap = tok_rows * top_count * 3 // (2 * local * ep_size)
    halves = tp_size // 2
    quarter_rows = tok_rows // tp_size
    half_rows = tok_rows // 2

    meta = jnp.concatenate([expert_ids.T.astype(bf16), route_weights.T], axis=0)
    meta_rows = jnp.pad(meta, ((0, 0), (0, width - tok_rows)))

    def share(start, rows):
        return jnp.concatenate(
            [
                lax.dynamic_slice_in_dim(tokens, start, rows, 0),
                lax.dynamic_slice_in_dim(cotangent, start, rows, 0),
                meta_rows,
            ],
            axis=0,
        )

    own_half = share((tp % 2) * half_rows, half_rows)
    own_quarter = share(((tp % 2) * halves + tp // 2) * quarter_rows, quarter_rows)
    pairs = ep_size // 2
    line = pairs == 4 and halves == 2
    middle = (ep // 2 == 1) | (ep // 2 == 2)

    def along(value, moves):
        return lax.ppermute(
            value, "ep", [(2 * a + i, 2 * b + i) for a, b in moves for i in range(2)]
        )

    far = [None] * pairs
    if line:
        far[1] = along(own_quarter, ((0, 1), (1, 0), (2, 3), (3, 2)))
        inner = along(own_quarter, ((1, 2), (2, 1)))
        far[2] = jnp.where(middle, inner, along(inner, ((1, 0), (2, 3))))
        inner = along(far[1], ((1, 2), (2, 1)))
        far[3] = jnp.where(middle, inner, along(inner, ((1, 0), (2, 3))))
    else:
        for k in range(1, pairs):
            far[k] = swap(own_quarter, "ep", 2 * k)
    near = [swap(own_half, "ep", 1)]
    near += [swap(far[k], "ep", 1) for k in range(1, pairs)]

    def gathered(value, whole):
        held = [(value, 0)]
        if not whole:
            held += [(swap(value, "tp", 2 * p), 2 * p) for p in range(1, halves)]
        held += [(swap(v, "tp", 1), mask ^ 1) for v, mask in tuple(held)]
        return [v for v, _ in held], tuple(mask for _, mask in held)

    blocks = [[([tokens, cotangent, meta], None), gathered(near[0], True)]]
    for k in range(1, pairs):
        blocks.append([gathered(far[k], False), gathered(near[k], False)])

    dense_g = dense_gate[None, :]
    dgrad = jnp.zeros(dense_weight.shape, f32)
    weights = (gate_weight, up_weight, down_weight)
    slabs = None
    results = {}
    for k in range(pairs):
        *slabs, keep, send, dgrad = expert_pair(
            blocks[k], weights, dense_weight, dense_g, dgrad, slabs, k, pairs, tok_rows, cap,
            top_count,
        )
        other = swap(send, "tp", 1)
        both = keep.astype(f32) + other.astype(f32)
        moved = swap(both[1].astype(bf16), "ep", 1)
        both = both[0] + moved.astype(f32)
        total = both[0]
        for h in range(1, halves):
            total = total + swap(both[h].astype(bf16), "tp", 2 * h).astype(f32)
        results[k] = total
    row, hid, gb, ub, wt = slabs
    grads = []
    for left, right in ((row, gb), (row, ub), (hid, wt)):
        grads.append(batched(left, right))
    grad_gate, grad_up, grad_down = grads

    total = results[0]
    for k in range(1, pairs):
        value = results[k].astype(bf16)
        if not line or k == 1:
            total = total + swap(value, "ep", 2 * k).astype(f32)
            continue
        straight, crossed = ((0, 2), (3, 1)), ((1, 2), (2, 1))
        if k == 3:
            straight, crossed = ((1, 3), (2, 0)), ((0, 3), (3, 0))
        total = total + along(value, straight).astype(f32)
        total = total + along(value, crossed).astype(f32)
    token_grad = total[:tok_rows].astype(bf16)
    weight_grad = total[tok_rows : tok_rows + top_count, :tok_rows].astype(bf16).T
    return (token_grad, weight_grad, grad_gate, grad_up, grad_down, dgrad)


def solution(mesh):
    in_specs = (
        P("ep", None),
        P("ep", None),
        P("ep", None),
        P("ep", None),
        P("ep", None, "tp"),
        P("ep", None, "tp"),
        P("ep", "tp", None),
        P("tp", "ep"),
        P(),
    )
    out_specs = (
        P("ep", "tp"),
        P("ep", None),
        P("ep", None, "tp"),
        P("ep", None, "tp"),
        P("ep", "tp", None),
        P("tp", "ep"),
    )

    return jax.shard_map(shards, mesh=mesh, in_specs=in_specs, out_specs=out_specs, check_vma=False)
```

time: 360 us -> 239 us (0.66); the launches traced: 354 us -> 239 us
  blocking collectives: 94.6 us -> 0 us
  Pallas kernels: 0 us -> 69.8 us
  local copies, waits for them, and re-layouts: 66.8 us -> 6.8 us
  starting transfers between devices: 13.9 us -> 45.6 us
  matrix products: 49.9 us -> 21.8 us
  other arithmetic: 28.4 us -> 5.1 us
  between operations: 16.4 us -> 1.39 us
  waiting for transfers between devices: 84.1 us -> 88.2 us
    ppermute x0 -> x45, waiting for transfers between devices: none -> 88.2 us  [the longest x36 65.6 us: swap(): return lax.ppermute(value, axis, [(i, i ^ mask) for i in range(size)])]
    all_to_all x2 -> x0, blocking collectives: 84.5 us -> none  [the longest x1 44.3 us: shards(): lax.all_to_all(cut_input, 'ep', split_axis=0, concat_axis=0, tiled=True)]
    pallas_call x0 -> x4, Pallas kernels: none -> 69.8 us  [expert_pair(): pl.pallas_call(functools.partial(pair_kernel, layout, local, cap), grid=(...]
    ppermute x0 -> x45, starting transfers between devices: none -> 45.6 us  [the longest x36 27.8 us: swap(): return lax.ppermute(value, axis, [(i, i ^ mask) for i in range(size)])]
    reduce_scatter x2 -> x0, waiting for transfers between devices: 41.7 us -> none  [the longest x1 29.3 us: shards(): lax.psum_scatter(back_terms.astype(jnp.bfloat16), 'tp', scatter_dimension...]
    gather x5 -> x0, local copies, waits for them, and re-layouts: 34.1 us -> none  [the longest x1 9.46 us: shards(): jnp.concatenate([route_weights.reshape(routed), jnp.zeros((1,), jnp.bfloa...]
    dot_general x18 -> x3, matrix products: 49.9 us -> 21.8 us  [batched(): lax.dot_general(lhs, rhs, (((1,), (1,)), ((0,), (0,))), preferred_element...]
    another operation x7 -> x1, other arithmetic: 24.4 us -> 0.25 us  [the longest x1 8.2 us: shards(): jnp.stack(gate_list)]
  transfers between devices with their start and end apart: 8 -> 45, of which waited for: 6 -> 11; matrix products, arithmetic and copies ran while one was open for 32% -> 12% of each run, Pallas kernels for 0% -> 29%
where the time goes in v1:
time: 239 us
  waiting for transfers between devices  88.2 us (37%)
  Pallas kernels  69.8 us (29%)
  starting transfers between devices  45.6 us (19%)
  matrix products  21.8 us (9%)
  local copies, waits for them, and re-layouts  6.8 us (3%)
  other arithmetic  5.1 us (2%)
    pallas_call x4, Pallas kernels, expert_pair(): pl.pallas_call(functools.partial(pair_kernel, layout, local, cap), grid=(...  69.8 us
    ppermute x36, waiting for transfers between devices, swap(): return lax.ppermute(value, axis, [(i, i ^ mask) for i in range(size)])  65.6 us
    ppermute x36, starting transfers between devices, swap(): return lax.ppermute(value, axis, [(i, i ^ mask) for i in range(size)])  27.8 us
    ppermute x9, waiting for transfers between devices, along(): lax.ppermute(value, 'ep', [(2 * a + i, 2 * b + i) for a, b in moves for i...  22.7 us
    dot_general x3, matrix products, batched(): lax.dot_general(lhs, rhs, (((1,), (1,)), ((0,), (0,))), preferred_element...  21.8 us
    ppermute x9, starting transfers between devices, along(): lax.ppermute(value, 'ep', [(2 * a + i, 2 * b + i) for a, b in moves for i...  17.8 us
  transfers between devices with their start and end apart: 45, of which 11 were waited for; matrix products, arithmetic and copies ran while one was open for 12% of the time, Pallas kernels for 29%

profile of v1, /device:TPU:0, one launch (start us, length us, event | category | flops | bytes accessed | tf_op | source)
XLA Modules:
  0.0 238.8 jit_solution(13196234853642709012)
XLA Ops:
  3.5 3.0 %collective-permute-start = (bf16[264,2048]{1,0:T(8,128)(2,1)S(1)}, bf16[264,2048]{1,0:T(8,128)(2,1)}, u32[]{:S(2)}, u32[]{:S(2)}) collective-permute-start(bf16[264,2048]{1,0:T(8,128)(2,1)S(1)} %pad_maximum_fusion), channel_id=1, source_target_pairs={{0,4},{4,0},{8,12},{12,8},{16,20},{20,16},{24,28},{28,24},{1,5},{5... | collective-permute-start | bytes 3244040 | tf_op jit(solution)/shard_map/ppermute | solution.py:18
  7.6 1.6 collective-permute-start.5
  10.7 11.0 %collective-permute-done.5.refs_0_ = bf16[136,2048]{1,0:T(8,128)(2,1)S(1)} collective-permute-done((bf16[136,2048]{1,0:T(8,128)(2,1)S(1)}, bf16[136,2048]{1,0:T(8,128)(2,1)S(1)}, u32[]{:S(2)}, u32[]{:S(2)}) %collective-permute-start.5) | collective-permute-done | bytes 557088 | tf_op jit(solution)/shard_map/ppermute | solution.py:293
  22.1 1.7 collective-permute-start.6
  25.2 6.1 %collective-permute-done.refs_3_ = bf16[264,2048]{1,0:T(8,128)(2,1)} collective-permute-done((bf16[264,2048]{1,0:T(8,128)(2,1)S(1)}, bf16[264,2048]{1,0:T(8,128)(2,1)}, u32[]{:S(2)}, u32[]{:S(2)}) %collective-permute-start) | collective-permute-done | bytes 1081376 | tf_op jit(solution)/shard_map/ppermute | solution.py:18
  32.0 10.3 %collective-permute-done.9.refs_4_ = bf16[136,2048]{1,0:T(8,128)(2,1)S(1)} collective-permute-done((bf16[136,2048]{1,0:T(8,128)(2,1)S(1)}, bf16[136,2048]{1,0:T(8,128)(2,1)S(1)}, u32[]{:S(2)}, u32[]{:S(2)}) %collective-permute-start.9) | collective-permute-done | bytes 557088 | tf_op jit(solution)/shard_map/ppermute | solution.py:18
  42.3 1.8 collective-permute-start.10
  47.3 8.9 %collective-permute-done.10.refs_5_ = bf16[136,2048]{1,0:T(8,128)(2,1)} collective-permute-done((bf16[136,2048]{1,0:T(8,128)(2,1)S(1)}, bf16[136,2048]{1,0:T(8,128)(2,1)}, u32[]{:S(2)}, u32[]{:S(2)}) %collective-permute-start.10) | collective-permute-done | bytes 557088 | tf_op jit(solution)/shard_map/ppermute | solution.py:18
  60.7 11.0 %collective-permute-done.19.refs_1_ = bf16[136,2048]{1,0:T(8,128)(2,1)S(1)} collective-permute-done((bf16[136,2048]{1,0:T(8,128)(2,1)S(1)}, bf16[136,2048]{1,0:T(8,128)(2,1)S(1)}, u32[]{:S(2)}, u32[]{:S(2)}) %collective-permute-start.19) | collective-permute-done | bytes 557088 | tf_op jit(solution)/shard_map/ppermute | solution.py:18
  73.9 7.2 %collective-permute-done.23.refs_5_ = bf16[136,2048]{1,0:T(8,128)(2,1)S(1)} collective-permute-done((bf16[136,2048]{1,0:T(8,128)(2,1)S(1)}, bf16[136,2048]{1,0:T(8,128)(2,1)S(1)}, u32[]{:S(2)}, u32[]{:S(2)}) %collective-permute-start.23) | collective-permute-done | bytes 557088 | tf_op jit(solution)/shard_map/ppermute | solution.py:18
  82.0 17.2 %expert_pair.4 = (bf16[2,768,2048]{2,1,0:T(8,128)(2,1)}, bf16[2,768,512]{2,1,0:T(8,128)(2,1)}, bf16[2,768,512]{2,1,0:T(8,128)(2,1)}, bf16[2,768,512]{2,1,0:T(8,1...) custom-call(bf16[256,2048]{1,0:T(8,128)(2,1)} %refs_0_.1, ...), custom_call_target="tpu_custom_call" | custom-call | flops 5637144576 | bytes 20971520 | tf_op jit(solution)/shard_map/expert_pair/pallas_call | solution.py:212
  101.0 17.3 %expert_pair.5 = (bf16[2,768,2048]{2,1,0:T(8,128)(2,1)}, bf16[2,768,512]{2,1,0:T(8,128)(2,1)}, bf16[2,768,512]{2,1,0:T(8,128)(2,1)}, bf16[2,768,512]{2,1,0:T(8,1...) custom-call(bf16[136,2048]{1,0:T(8,128)(2,1)} %copy-done.9, ...), custom_call_target="tpu_custom_call", output_to_operand_aliasing={{0}: (14, {}), {1}: (15, {}), {2}: (16, {}), {3}: (17, {}),... | custom-call | flops 5637144576 | bytes 20971520 | tf_op jit(solution)/shard_map/expert_pair/pallas_call | solution.py:212
  119.9 17.6 %expert_pair.6 = (bf16[2,768,2048]{2,1,0:T(8,128)(2,1)}, bf16[2,768,512]{2,1,0:T(8,128)(2,1)}, bf16[2,768,512]{2,1,0:T(8,128)(2,1)}, bf16[2,768,512]{2,1,0:T(8,1...) custom-call(bf16[136,2048]{1,0:T(8,128)(2,1)} %copy-done.4, ...), custom_call_target="tpu_custom_call", output_to_operand_aliasing={{0}: (14, {}), {1}: (15, {}), {2}: (16, {}), {3}: (17, {}),... | custom-call | flops 5637144576 | bytes 20971520 | tf_op jit(solution)/shard_map/expert_pair/pallas_call | solution.py:212
  143.2 17.6 %expert_pair.7 = (bf16[2,768,2048]{2,1,0:T(8,128)(2,1)}, bf16[2,768,512]{2,1,0:T(8,128)(2,1)}, bf16[2,768,512]{2,1,0:T(8,128)(2,1)}, bf16[2,768,512]{2,1,0:T(8,1...) custom-call(bf16[136,2048]{1,0:T(8,128)(2,1)} %copy-done.3, ...), custom_call_target="tpu_custom_call", output_to_operand_aliasing={{0}: (14, {}), {1}: (15, {}), {2}: (16, {}), {3}: (17, {}),... | custom-call | flops 5637144576 | bytes 20971520 | tf_op jit(solution)/shard_map/expert_pair/pallas_call | solution.py:212
  160.8 10.2 %fusion.26 = f32[2,2048,512]{2,1,0:T(8,128)} fusion(bf16[2,768,2048]{2,1,0:T(8,128)(2,1)} %get-tuple-element.64, bf16[2,768,512]{2,1,0:T(8,128)(2,1)} %get-tuple-element.66), kind=kOutput, calls=%fused_computation.57 | convolution fusion | flops 3221225472 | bytes 16252928 | tf_op jit(solution)/shard_map/dot_general | solution.py:248
  171.1 5.8 %fusion.25 = f32[2,2048,512]{2,1,0:T(8,128)} fusion(bf16[2,768,2048]{2,1,0:T(8,128)(2,1)S(1)} %copy-done, bf16[2,768,512]{2,1,0:T(8,128)(2,1)S(1)} %copy-done.2), kind=kOutput, calls=%fused_computation.56 | convolution fusion | flops 3221225472 | bytes 16252928 | tf_op jit(solution)/shard_map/dot_general | solution.py:248
  179.0 1.6 collective-permute-start.27
  183.2 11.1 %collective-permute-done.27 = bf16[2,264,512]{2,1,0:T(8,128)(2,1)S(1)} collective-permute-done((bf16[2,264,512]{2,1,0:T(8,128)(2,1)S(1)}, bf16[2,264,512]{2,1,0:T(8,128)(2,1)S(1)}, u32[]{:S(2)}, u32[]{:S(2)}) %collective-permute-start.27) | collective-permute-done | bytes 540704 | tf_op jit(solution)/shard_map/ppermute | solution.py:18
  195.4 9.6 %collective-permute-done.41 = bf16[2,264,512]{2,1,0:T(8,128)(2,1)S(1)} collective-permute-done((bf16[2,264,512]{2,1,0:T(8,128)(2,1)S(1)}, bf16[2,264,512]{2,1,0:T(8,128)(2,1)S(1)}, u32[]{:S(2)}, u32[]{:S(2)}) %collective-permute-start.41) | collective-permute-done | bytes 540704 | tf_op jit(solution)/shard_map/ppermute | solution.py:18
  206.6 1.7 collective-permute-start.16
  208.4 4.5 %collective-permute-start.29 = (bf16[264,512]{1,0:T(8,128)(2,1)S(1)}, bf16[264,512]{1,0:T(8,128)(2,1)S(1)}, u32[]{:S(2)}, u32[]{:S(2)}) collective-permute-start(bf16[264,512]{1,0:T(8,128)(2,1)S(1)} %fusion.11), channel_id=1, source_target_pairs={{0,16},{4,20},{24,8},{28,12},{1,17},{5,21},{25,9},{29,13},{2,18},{... | collective-permute-start | bytes 811016 | tf_op jit(solution)/shard_map/ppermute | solution.py:293
  215.0 5.0 %collective-permute-start.44 = (bf16[264,512]{1,0:T(8,128)(2,1)S(1)}, bf16[264,512]{1,0:T(8,128)(2,1)S(1)}, u32[]{:S(2)}, u32[]{:S(2)}) collective-permute-start(bf16[264,512]{1,0:T(8,128)(2,1)S(1)} %fusion.9), channel_id=1, source_target_pairs={{0,24},{4,28},{24,0},{28,4},{1,25},{5,29},{25,1},{29,5},{2,26},{6,... | collective-permute-start | bytes 811016 | tf_op jit(solution)/shard_map/ppermute | solution.py:293
  220.0 5.8 %fusion.27 = f32[2,512,2048]{2,1,0:T(8,128)} fusion(bf16[2,768,512]{2,1,0:T(8,128)(2,1)S(1)} %copy-done.1, bf16[2,768,2048]{2,1,0:T(8,128)(2,1)S(1)} %bitcast.79), kind=kOutput, calls=%fused_computation.58 | convolution fusion | flops 3221225472 | bytes 16252928 | tf_op jit(solution)/shard_map/dot_general | solution.py:248
  225.8 11.4 %collective-permute-done.43 = bf16[264,512]{1,0:T(8,128)(2,1)S(1)} collective-permute-done((bf16[264,512]{1,0:T(8,128)(2,1)S(1)}, bf16[264,512]{1,0:T(8,128)(2,1)S(1)}, u32[]{:S(2)}, u32[]{:S(2)}) %collective-permute-start.43) | collective-permute-done | bytes 270368 | tf_op jit(solution)/shard_map/ppermute | solution.py:293
  (164 shorter events, 38.3 us)
Async XLA Ops:
  3.5 27.9 %collective-permute-start = (bf16[264,2048]{1,0:T(8,128)(2,1)S(1)}, bf16[264,2048]{1,0:T(8,128)(2,1)}, u32[]{:S(2)}, u32[]{:S(2)}) collective-permute-start(bf16[264,2048]{1,0:T(8,128)(2,1)S(1)} %pad_maximum_fusion), channel_id=1, source_target_pairs={{0,4},{4,0},{8,12},{12,8},{16,20},{20,16},{24,28},{28,24},{1,5},{5... | collective-permute-start | bytes 3244040 | tf_op jit(solution)/shard_map/ppermute | solution.py:18
  21.8 20.5 %collective-permute-start.9 = (bf16[136,2048]{1,0:T(8,128)(2,1)S(1)}, bf16[136,2048]{1,0:T(8,128)(2,1)S(1)}, u32[]{:S(2)}, u32[]{:S(2)}) collective-permute-start(bf16[136,2048]{1,0:T(8,128)(2,1)S(1)} %collective-permute-done.5.refs_0_), channel_id=1, source_target_pairs={{0,4},{4,0},{8,12},{12,8},{16,20},{20,16},{24,28},{28,24},{1,5},{5... | collective-permute-start | bytes 1671176 | tf_op jit(solution)/shard_map/ppermute | solution.py:18
  22.1 21.9 %collective-permute-start.6 = (bf16[136,2048]{1,0:T(8,128)(2,1)S(1)}, bf16[136,2048]{1,0:T(8,128)(2,1)S(1)}, u32[]{:S(2)}, u32[]{:S(2)}) collective-permute-start(bf16[136,2048]{1,0:T(8,128)(2,1)S(1)} %collective-permute-done.5.refs_0_), channel_id=1, source_target_pairs={{0,2},{1,3},{2,0},{3,1},{4,6},{5,7},{6,4},{7,5},{8,10},{9,11},{10,... | collective-permute-start | bytes 1671176 | tf_op jit(solution)/shard_map/ppermute | solution.py:18
  25.1 20.6 %collective-permute-start.7 = (bf16[136,2048]{1,0:T(8,128)(2,1)S(1)}, bf16[136,2048]{1,0:T(8,128)(2,1)S(1)}, u32[]{:S(2)}, u32[]{:S(2)}) collective-permute-start(bf16[136,2048]{1,0:T(8,128)(2,1)S(1)} %collective-permute-done.5.refs_0_), channel_id=1, source_target_pairs={{0,1},{1,0},{2,3},{3,2},{4,5},{5,4},{6,7},{7,6},{8,9},{9,8},{10,11... | collective-permute-start | bytes 1671176 | tf_op jit(solution)/shard_map/ppermute | solution.py:18
  47.3 26.6 %collective-permute-start.1 = (bf16[264,2048]{1,0:T(8,128)(2,1)}, bf16[264,2048]{1,0:T(8,128)(2,1)S(1)}, u32[]{:S(2)}, u32[]{:S(2)}) collective-permute-start(bf16[264,2048]{1,0:T(8,128)(2,1)} %collective-permute-done.refs_3_), channel_id=1, source_target_pairs={{0,1},{1,0},{2,3},{3,2},{4,5},{5,4},{6,7},{7,6},{8,9},{9,8},{10,11... | collective-permute-start | bytes 3244040 | tf_op jit(solution)/shard_map/ppermute | solution.py:18
  60.4 20.7 %collective-permute-start.23 = (bf16[136,2048]{1,0:T(8,128)(2,1)S(1)}, bf16[136,2048]{1,0:T(8,128)(2,1)S(1)}, u32[]{:S(2)}, u32[]{:S(2)}) collective-permute-start(bf16[136,2048]{1,0:T(8,128)(2,1)S(1)} %collective-permute-done.22.refs_4_), channel_id=1, source_target_pairs={{0,2},{1,3},{2,0},{3,1},{4,6},{5,7},{6,4},{7,5},{8,10},{9,11},{10,... | collective-permute-start | bytes 1671176 | tf_op jit(solution)/shard_map/ppermute | solution.py:18
  71.7 27.6 %collective-permute-start.12 = (bf16[136,2048]{1,0:T(8,128)(2,1)}, bf16[136,2048]{1,0:T(8,128)(2,1)S(1)}, u32[]{:S(2)}, u32[]{:S(2)}) collective-permute-start(bf16[136,2048]{1,0:T(8,128)(2,1)} %collective-permute-done.10.refs_5_), channel_id=1, source_target_pairs={{0,1},{1,0},{2,3},{3,2},{4,5},{5,4},{6,7},{7,6},{8,9},{9,8},{10,11... | collective-permute-start | bytes 1671176 | tf_op jit(solution)/shard_map/ppermute | solution.py:18
  71.9 27.9 %collective-permute-start.21 = (bf16[136,2048]{1,0:T(8,128)(2,1)S(1)}, bf16[136,2048]{1,0:T(8,128)(2,1)}, u32[]{:S(2)}, u32[]{:S(2)}) collective-permute-start(bf16[136,2048]{1,0:T(8,128)(2,1)S(1)} %collective-permute-done.19.refs_1_), channel_id=1, source_target_pairs={{0,1},{1,0},{2,3},{3,2},{4,5},{5,4},{6,7},{7,6},{8,9},{9,8},{10,11... | collective-permute-start | bytes 1671176 | tf_op jit(solution)/shard_map/ppermute | solution.py:18
  72.3 46.2 %collective-permute-start.36 = (bf16[136,2048]{1,0:T(8,128)(2,1)S(1)}, bf16[136,2048]{1,0:T(8,128)(2,1)}, u32[]{:S(2)}, u32[]{:S(2)}) collective-permute-start(bf16[136,2048]{1,0:T(8,128)(2,1)S(1)} %broadcast_select_fusion.refs_0_), channel_id=1, source_target_pairs={{0,4},{4,0},{8,12},{12,8},{16,20},{20,16},{24,28},{28,24},{1,5},{5... | collective-permute-start | bytes 1671176 | tf_op jit(solution)/shard_map/ppermute | solution.py:18
  73.8 44.6 %collective-permute-start.24 = (bf16[136,2048]{1,0:T(8,128)(2,1)S(1)}, bf16[136,2048]{1,0:T(8,128)(2,1)S(1)}, u32[]{:S(2)}, u32[]{:S(2)}) collective-permute-start(bf16[136,2048]{1,0:T(8,128)(2,1)S(1)} %collective-permute-done.22.refs_4_), channel_id=1, source_target_pairs={{0,1},{1,0},{2,3},{3,2},{4,5},{5,4},{6,7},{7,6},{8,9},{9,8},{10,11... | collective-permute-start | bytes 1671176 | tf_op jit(solution)/shard_map/ppermute | solution.py:18
  81.1 38.0 %collective-permute-start.25 = (bf16[136,2048]{1,0:T(8,128)(2,1)S(1)}, bf16[136,2048]{1,0:T(8,128)(2,1)S(1)}, u32[]{:S(2)}, u32[]{:S(2)}) collective-permute-start(bf16[136,2048]{1,0:T(8,128)(2,1)S(1)} %collective-permute-done.23.refs_5_), channel_id=1, source_target_pairs={{0,1},{1,0},{2,3},{3,2},{4,5},{5,4},{6,7},{7,6},{8,9},{9,8},{10,11... | collective-permute-start | bytes 1671176 | tf_op jit(solution)/shard_map/ppermute | solution.py:18
  99.3 38.3 %collective-permute-start.2 = (bf16[2,2,264,512]{3,2,1,0:T(8,128)(2,1)}, bf16[2,2,264,512]{3,2,1,0:T(8,128)(2,1)S(1)}, u32[]{:S(2)}, u32[]{:S(2)}) collective-permute-start(bf16[2,2,264,512]{3,2,1,0:T(8,128)(2,1)} %get-tuple-element.39), channel_id=1, source_target_pairs={{0,1},{1,0},{2,3},{3,2},{4,5},{5,4},{6,7},{7,6},{8,9},{9,8},{10,11... | collective-permute-start | bytes 3244040 | tf_op jit(solution)/shard_map/ppermute | solution.py:18
  99.8 37.7 %collective-permute-start.33 = (bf16[136,2048]{1,0:T(8,128)(2,1)S(1)}, bf16[136,2048]{1,0:T(8,128)(2,1)S(1)}, u32[]{:S(2)}, u32[]{:S(2)}) collective-permute-start(bf16[136,2048]{1,0:T(8,128)(2,1)S(1)} %broadcast_select_fusion.refs_0_), channel_id=1, source_target_pairs={{0,2},{1,3},{2,0},{3,1},{4,6},{5,7},{6,4},{7,5},{8,10},{9,11},{10,... | collective-permute-start | bytes 1671176 | tf_op jit(solution)/shard_map/ppermute | solution.py:18
  118.4 21.8 %collective-permute-start.34 = (bf16[136,2048]{1,0:T(8,128)(2,1)S(1)}, bf16[136,2048]{1,0:T(8,128)(2,1)S(1)}, u32[]{:S(2)}, u32[]{:S(2)}) collective-permute-start(bf16[136,2048]{1,0:T(8,128)(2,1)S(1)} %broadcast_select_fusion.refs_0_), channel_id=1, source_target_pairs={{0,1},{1,0},{2,3},{3,2},{4,5},{5,4},{6,7},{7,6},{8,9},{9,8},{10,11... | collective-permute-start | bytes 1671176 | tf_op jit(solution)/shard_map/ppermute | solution.py:18
  118.5 20.9 %collective-permute-start.13 = (bf16[2,2,264,512]{3,2,1,0:T(8,128)(2,1)}, bf16[2,2,264,512]{3,2,1,0:T(8,128)(2,1)S(1)}, u32[]{:S(2)}, u32[]{:S(2)}) collective-permute-start(bf16[2,2,264,512]{3,2,1,0:T(8,128)(2,1)} %get-tuple-element.47), channel_id=1, source_target_pairs={{0,1},{1,0},{2,3},{3,2},{4,5},{5,4},{6,7},{7,6},{8,9},{9,8},{10,11... | collective-permute-start | bytes 3244040 | tf_op jit(solution)/shard_map/ppermute | solution.py:18
  119.0 20.3 %collective-permute-start.37 = (bf16[136,2048]{1,0:T(8,128)(2,1)}, bf16[136,2048]{1,0:T(8,128)(2,1)}, u32[]{:S(2)}, u32[]{:S(2)}) collective-permute-start(bf16[136,2048]{1,0:T(8,128)(2,1)} %collective-permute-done.36.refs_4_), channel_id=1, source_target_pairs={{0,2},{1,3},{2,0},{3,1},{4,6},{5,7},{6,4},{7,5},{8,10},{9,11},{10,... | collective-permute-start | bytes 1671176 | tf_op jit(solution)/shard_map/ppermute | solution.py:18
  139.3 39.3 %collective-permute-start.26 = (bf16[2,2,264,512]{3,2,1,0:T(8,128)(2,1)}, bf16[2,2,264,512]{3,2,1,0:T(8,128)(2,1)S(1)}, u32[]{:S(2)}, u32[]{:S(2)}) collective-permute-start(bf16[2,2,264,512]{3,2,1,0:T(8,128)(2,1)} %get-tuple-element.55), channel_id=1, source_target_pairs={{0,1},{1,0},{2,3},{3,2},{4,5},{5,4},{6,7},{7,6},{8,9},{9,8},{10,11... | collective-permute-start | bytes 3244040 | tf_op jit(solution)/shard_map/ppermute | solution.py:18
  140.3 36.6 %collective-permute-start.3 = (bf16[2,264,512]{2,1,0:T(8,128)(2,1)}, bf16[2,264,512]{2,1,0:T(8,128)(2,1)S(1)}, u32[]{:S(2)}, u32[]{:S(2)}) collective-permute-start(bf16[2,264,512]{2,1,0:T(8,128)(2,1)} %fusion.4), channel_id=1, source_target_pairs={{0,4},{4,0},{8,12},{12,8},{16,20},{20,16},{24,28},{28,24},{1,5},{5... | collective-permute-start | bytes 1622024 | tf_op jit(solution)/shard_map/ppermute | solution.py:18
  142.5 35.9 %collective-permute-start.14 = (bf16[2,264,512]{2,1,0:T(8,128)(2,1)S(1)}, bf16[2,264,512]{2,1,0:T(8,128)(2,1)S(1)}, u32[]{:S(2)}, u32[]{:S(2)}) collective-permute-start(bf16[2,264,512]{2,1,0:T(8,128)(2,1)S(1)} %fusion.5), channel_id=1, source_target_pairs={{0,4},{4,0},{8,12},{12,8},{16,20},{20,16},{24,28},{28,24},{1,5},{5... | collective-permute-start | bytes 1622024 | tf_op jit(solution)/shard_map/ppermute | solution.py:18
  177.2 37.8 %collective-permute-start.4 = (bf16[264,512]{1,0:T(8,128)(2,1)S(1)}, bf16[264,512]{1,0:T(8,128)(2,1)S(1)}, u32[]{:S(2)}, u32[]{:S(2)}) collective-permute-start(bf16[264,512]{1,0:T(8,128)(2,1)S(1)} %fusion.21), channel_id=1, source_target_pairs={{0,2},{1,3},{2,0},{3,1},{4,6},{5,7},{6,4},{7,5},{8,10},{9,11},{10,... | collective-permute-start | bytes 811016 | tf_op jit(solution)/shard_map/ppermute | solution.py:18
  181.0 24.0 %collective-permute-start.41 = (bf16[2,264,512]{2,1,0:T(8,128)(2,1)S(1)}, bf16[2,264,512]{2,1,0:T(8,128)(2,1)S(1)}, u32[]{:S(2)}, u32[]{:S(2)}) collective-permute-start(bf16[2,264,512]{2,1,0:T(8,128)(2,1)S(1)} %fusion.7), channel_id=1, source_target_pairs={{0,4},{4,0},{8,12},{12,8},{16,20},{20,16},{24,28},{28,24},{1,5},{5... | collective-permute-start | bytes 1622024 | tf_op jit(solution)/shard_map/ppermute | solution.py:18
  182.2 24.3 %collective-permute-start.15 = (bf16[264,512]{1,0:T(8,128)(2,1)S(1)}, bf16[264,512]{1,0:T(8,128)(2,1)S(1)}, u32[]{:S(2)}, u32[]{:S(2)}) collective-permute-start(bf16[264,512]{1,0:T(8,128)(2,1)S(1)} %fusion.22), channel_id=1, source_target_pairs={{0,2},{1,3},{2,0},{3,1},{4,6},{5,7},{6,4},{7,5},{8,10},{9,11},{10,... | collective-permute-start | bytes 811016 | tf_op jit(solution)/shard_map/ppermute | solution.py:18
  213.7 23.5 %collective-permute-start.43 = (bf16[264,512]{1,0:T(8,128)(2,1)S(1)}, bf16[264,512]{1,0:T(8,128)(2,1)S(1)}, u32[]{:S(2)}, u32[]{:S(2)}) collective-permute-start(bf16[264,512]{1,0:T(8,128)(2,1)S(1)} %fusion.9), channel_id=1, source_target_pairs={{8,24},{12,28},{16,0},{20,4},{9,25},{13,29},{17,1},{21,5},{10,26},... | collective-permute-start | bytes 811016 | tf_op jit(solution)/shard_map/ppermute | solution.py:293
  215.0 22.2 %collective-permute-start.44 = (bf16[264,512]{1,0:T(8,128)(2,1)S(1)}, bf16[264,512]{1,0:T(8,128)(2,1)S(1)}, u32[]{:S(2)}, u32[]{:S(2)}) collective-permute-start(bf16[264,512]{1,0:T(8,128)(2,1)S(1)} %fusion.9), channel_id=1, source_target_pairs={{0,24},{4,28},{24,0},{28,4},{1,25},{5,29},{25,1},{29,5},{2,26},{6,... | collective-permute-start | bytes 811016 | tf_op jit(solution)/shard_map/ppermute | solution.py:293
  (50 other events, 841.6 us)

commit v2 on v1

--- a/solution.py
+++ b/solution.py
@@ -26,10 +26,11 @@
     return lax.dot_general(lhs, rhs, (((0,), (0,)), ((), ())), preferred_element_type=f32)
 
 
-def pair_kernel(layout, local, cap, *refs):
+def pair_kernel(layout, local, cap, fresh, *refs):
     count = len(layout)
     inputs, refs = refs[: sum(n for n, _ in layout)], refs[sum(n for n, _ in layout) :]
-    stored, (dense_w_ref, dense_g_ref, dgrad_in) = refs[:3], refs[3:6]
+    stored, (dense_w_ref, dense_g_ref) = refs[:3], refs[3:5]
+    dgrad_in = None if fresh else refs[5]
     held, (weight_sems, block, meta, picks, rows_s, cots_s, back, dense, score_total, sems) = (
         refs[-13:-10], refs[-10:]
     )
@@ -97,7 +98,7 @@
         out_part, in_part = dense_w_ref.shape[1], dense_w_ref.shape[0]
         own_cols = pl.ds(pl.multiple_of(tp * in_part, 128), in_part)
         out_cols = pl.ds(pl.multiple_of(ep * out_part, 128), out_part)
-        dense_sum = dgrad_in[...]
+        dense_sum = jnp.zeros(dgrad_ref.shape, f32) if fresh else dgrad_in[...]
         for b in range(count):
             for copy in copies[counts[b] : counts[b + 1]]:
                 copy.wait()
@@ -188,7 +189,7 @@
 
 
 def expert_pair(
-    blocks, weights, dense_w, dense_g, dgrad, slabs, index, count_all, tok_rows, cap, top
+    blocks, weights, dense_w, dense_g, dgrad, slabs, first, count_all, tok_rows, cap, top
 ):
     local, width, units = weights[0].shape
     count = len(blocks)
@@ -200,23 +201,23 @@
     arrays = [v for values, _ in blocks for v in values]
     layout = tuple((len(values), masks) for values, masks in blocks)
     payload = jax.ShapeDtypeStruct((count, halves, tok_rows + 8, part), bf16)
-    window = lambda lanes: pl.BlockSpec((1, m, lanes), lambda e: (e, index, 0))
+    window = lambda lanes: pl.BlockSpec((1, m, lanes), lambda e: (e, first // count, 0))
     slab_lanes = (width, units, units, units, width)
-    operands = [*arrays, *weights, dense_w, dense_g, dgrad]
-    specs = [hbm] * (len(arrays) + 3) + [vmem] * 3
+    operands = [*arrays, *weights, dense_w, dense_g]
+    specs = [hbm] * (len(arrays) + 3) + [vmem] * 2
     aliases = {}
     if slabs is not None:
-        aliases = {len(operands) + i: i for i in range(5)}
-        operands += list(slabs)
-        specs += [hbm] * 5
+        aliases = {len(operands) + 1 + i: i for i in range(5)}
+        operands += [dgrad, *slabs]
+        specs += [vmem] + [hbm] * 5
     return pl.pallas_call(
-        functools.partial(pair_kernel, layout, local, cap),
+        functools.partial(pair_kernel, layout, local, cap, slabs is None),
         grid=(local,),
         out_shape=(
-            *[jax.ShapeDtypeStruct((local, count_all * m, n), bf16) for n in slab_lanes],
+            *[jax.ShapeDtypeStruct((local, count_all * cap, n), bf16) for n in slab_lanes],
             payload,
             payload,
-            jax.ShapeDtypeStruct(dgrad.shape, f32),
+            jax.ShapeDtypeStruct(dense_w.shape, f32),
         ),
         in_specs=specs,
         out_specs=(*[window(n) for n in slab_lanes], vmem, vmem, vmem),
@@ -244,6 +245,12 @@
     )(*operands)
 
 
+def groups_of(ep_size, halves):
+    if ep_size == 8 and halves == 2:
+        return ((0, 1, 2), 0), ((3, 4, 5), 3), ((6, 7), 6)
+    return tuple(((b, b + 1), b) for b in range(0, ep_size, 2))
+
+
 def batched(lhs, rhs):
     return lax.dot_general(lhs, rhs, (((1,), (1,)), ((0,), (0,))), preferred_element_type=f32)
 
@@ -319,19 +326,22 @@
         blocks.append([gathered(far[k], False), gathered(near[k], False)])
 
     dense_g = dense_gate[None, :]
-    dgrad = jnp.zeros(dense_weight.shape, f32)
+    dgrad = None
     weights = (gate_weight, up_weight, down_weight)
     slabs = None
-    results = {}
+    results, summed = {}, {}
+    flat = [block for pair in blocks for block in pair]
+    for members, first in groups_of(ep_size, halves):
+        *slabs, keep, send, dgrad = expert_pair(
+            [flat[b] for b in members], weights, dense_weight, dense_g, dgrad, slabs, first,
+            ep_size, tok_rows, cap, top_count,
+        )
+        other = swap(send, "tp", 1)
+        held = [(keep[i].astype(f32) + other[i].astype(f32)).astype(bf16) for i in range(len(members))]
+        summed.update(zip(members, lax.optimization_barrier(held)))
     for k in range(pairs):
-        *slabs, keep, send, dgrad = expert_pair(
-            blocks[k], weights, dense_weight, dense_g, dgrad, slabs, k, pairs, tok_rows, cap,
-            top_count,
-        )
-        other = swap(send, "tp", 1)
-        both = keep.astype(f32) + other.astype(f32)
-        moved = swap(both[1].astype(bf16), "ep", 1)
-        both = both[0] + moved.astype(f32)
+        moved = swap(summed[2 * k + 1], "ep", 1)
+        both = summed[2 * k].astype(f32) + moved.astype(f32)
         total = both[0]
         for h in range(1, halves):
             total = total + swap(both[h].astype(bf16), "tp", 2 * h).astype(f32)

time: 239 us -> 238 us (level)
  waiting for transfers between devices: 88.2 us -> 102 us
  Pallas kernels: 69.8 us -> 57.3 us
    ppermute x36 -> x35, waiting for transfers between devices: 65.6 us -> 79.4 us  [swap(): return lax.ppermute(value, axis, [(i, i ^ mask) for i in range(size)])]
    pallas_call x4 -> x3, Pallas kernels: 69.8 us -> 57.3 us  [expert_pair(): pl.pallas_call(functools.partial(pair_kernel, layout, local, cap, slabs i...]
    ppermute x36 -> x35, starting transfers between devices: 27.8 us -> 24.5 us  [swap(): return lax.ppermute(value, axis, [(i, i ^ mask) for i in range(size)])]
  transfers between devices with their start and end apart: 45 -> 44, of which waited for: 11 -> 13; matrix products, arithmetic and copies ran while one was open for 12% -> 10% of each run, Pallas kernels for 29% -> 24%
where the time goes in v2:
time: 238 us; the launch traced here: 237 us
  waiting for transfers between devices  102 us (43%)
  Pallas kernels  57.3 us (24%)
  starting transfers between devices  43.6 us (18%)
  matrix products  21.8 us (9%)
  local copies, waits for them, and re-layouts  5.84 us (2%)
  other arithmetic  4.87 us (2%)
    ppermute x35, waiting for transfers between devices, swap(): return lax.ppermute(value, axis, [(i, i ^ mask) for i in range(size)])  79.4 us
    pallas_call x3, Pallas kernels, expert_pair(): pl.pallas_call(functools.partial(pair_kernel, layout, local, cap, slabs i...  57.3 us
    ppermute x35, starting transfers between devices, swap(): return lax.ppermute(value, axis, [(i, i ^ mask) for i in range(size)])  24.5 us
    ppermute x9, waiting for transfers between devices, along(): lax.ppermute(value, 'ep', [(2 * a + i, 2 * b + i) for a, b in moves for i...  23 us
    dot_general x3, matrix products, batched(): lax.dot_general(lhs, rhs, (((1,), (1,)), ((0,), (0,))), preferred_element...  21.8 us
    ppermute x9, starting transfers between devices, along(): lax.ppermute(value, 'ep', [(2 * a + i, 2 * b + i) for a, b in moves for i...  19.1 us
  transfers between devices with their start and end apart: 44, of which 13 were waited for; matrix products, arithmetic and copies ran while one was open for 10% of the time, Pallas kernels for 24%

profile of v2, /device:TPU:0, one launch (start us, length us, event | category | flops | bytes accessed | tf_op | source)
XLA Modules:
  0.0 237.2 jit_solution(15872196257633135805)
XLA Ops:
  4.1 3.1 %collective-permute-start.2 = (bf16[136,2048]{1,0:T(8,128)(2,1)}, bf16[136,2048]{1,0:T(8,128)(2,1)}, u32[]{:S(2)}, u32[]{:S(2)}) collective-permute-start(bf16[136,2048]{1,0:T(8,128)(2,1)} %pad_maximum_fusion.1), channel_id=1, source_target_pairs={{0,8},{4,12},{8,0},{12,4},{16,24},{20,28},{24,16},{28,20},{1,9},{5... | collective-permute-start | bytes 1671176 | tf_op jit(solution)/shard_map/ppermute | solution.py:300
  8.8 1.6 collective-permute-start
  10.4 9.8 %collective-permute-done.2.refs_5_ = bf16[136,2048]{1,0:T(8,128)(2,1)} collective-permute-done((bf16[136,2048]{1,0:T(8,128)(2,1)}, bf16[136,2048]{1,0:T(8,128)(2,1)}, u32[]{:S(2)}, u32[]{:S(2)}) %collective-permute-start.2) | collective-permute-done | bytes 557088 | tf_op jit(solution)/shard_map/ppermute | solution.py:300
  20.1 1.7 collective-permute-start.3
  23.9 10.2 %collective-permute-done.3.refs_6_ = bf16[136,2048]{1,0:T(8,128)(2,1)S(1)} collective-permute-done((bf16[136,2048]{1,0:T(8,128)(2,1)}, bf16[136,2048]{1,0:T(8,128)(2,1)S(1)}, u32[]{:S(2)}, u32[]{:S(2)}) %collective-permute-start.3) | collective-permute-done | bytes 557088 | tf_op jit(solution)/shard_map/ppermute | solution.py:18
  35.5 2.6 %collective-permute-done.14 = bf16[136,2048]{1,0:T(8,128)(2,1)S(1)} collective-permute-done((bf16[136,2048]{1,0:T(8,128)(2,1)}, bf16[136,2048]{1,0:T(8,128)(2,1)S(1)}, u32[]{:S(2)}, u32[]{:S(2)}) %collective-permute-start.14) | collective-permute-done | bytes 557088 | tf_op jit(solution)/shard_map/ppermute | solution.py:300
  41.1 1.6 collective-permute-start.15
  42.7 7.2 %collective-permute-done.9.refs_0_ = bf16[136,2048]{1,0:T(8,128)(2,1)S(1)} collective-permute-done((bf16[136,2048]{1,0:T(8,128)(2,1)}, bf16[136,2048]{1,0:T(8,128)(2,1)S(1)}, u32[]{:S(2)}, u32[]{:S(2)}) %collective-permute-start.9) | collective-permute-done | bytes 557088 | tf_op jit(solution)/shard_map/ppermute | solution.py:18
  51.3 8.0 %collective-permute-done.18.refs_8_ = bf16[136,2048]{1,0:T(8,128)(2,1)S(1)} collective-permute-done((bf16[136,2048]{1,0:T(8,128)(2,1)S(1)}, bf16[136,2048]{1,0:T(8,128)(2,1)S(1)}, u32[]{:S(2)}, u32[]{:S(2)}) %collective-permute-start.18) | collective-permute-done | bytes 557088 | tf_op jit(solution)/shard_map/ppermute | solution.py:18
  61.2 7.4 %collective-permute-done.10.refs_1_ = bf16[136,2048]{1,0:T(8,128)(2,1)S(1)} collective-permute-done((bf16[136,2048]{1,0:T(8,128)(2,1)S(1)}, bf16[136,2048]{1,0:T(8,128)(2,1)S(1)}, u32[]{:S(2)}, u32[]{:S(2)}) %collective-permute-start.10) | collective-permute-done | bytes 557088 | tf_op jit(solution)/shard_map/ppermute | solution.py:18
  70.7 9.9 %collective-permute-done.19.refs_9_ = bf16[136,2048]{1,0:T(8,128)(2,1)S(1)} collective-permute-done((bf16[136,2048]{1,0:T(8,128)(2,1)S(1)}, bf16[136,2048]{1,0:T(8,128)(2,1)S(1)}, u32[]{:S(2)}, u32[]{:S(2)}) %collective-permute-start.19) | collective-permute-done | bytes 557088 | tf_op jit(solution)/shard_map/ppermute | solution.py:18
  83.3 19.8 %expert_pair.3 = (bf16[2,768,2048]{2,1,0:T(8,128)(2,1)}, bf16[2,768,512]{2,1,0:T(8,128)(2,1)}, bf16[2,768,512]{2,1,0:T(8,128)(2,1)}, bf16[2,768,512]{2,1,0:T(8,1...) custom-call(bf16[256,2048]{1,0:T(8,128)(2,1)} %refs_0_.1, ...), custom_call_target="tpu_custom_call" | custom-call | flops 8455716864 | bytes 20971520 | tf_op jit(solution)/shard_map/expert_pair/pallas_call | solution.py:213
  106.0 20.0 %expert_pair.4 = (bf16[2,768,2048]{2,1,0:T(8,128)(2,1)}, bf16[2,768,512]{2,1,0:T(8,128)(2,1)}, bf16[2,768,512]{2,1,0:T(8,128)(2,1)}, bf16[2,768,512]{2,1,0:T(8,1...) custom-call(bf16[136,2048]{1,0:T(8,128)(2,1)} %copy-done.10, ...), custom_call_target="tpu_custom_call", output_to_operand_aliasing={{0}: (18, {}), {1}: (19, {}), {2}: (20, {}), {3}: (21, {}),... | custom-call | flops 8455716864 | bytes 20971520 | tf_op jit(solution)/shard_map/expert_pair/pallas_call | solution.py:213
  127.6 17.5 %expert_pair.5 = (bf16[2,768,2048]{2,1,0:T(8,128)(2,1)}, bf16[2,768,512]{2,1,0:T(8,128)(2,1)}, bf16[2,768,512]{2,1,0:T(8,128)(2,1)}, bf16[2,768,512]{2,1,0:T(8,1...) custom-call(bf16[136,2048]{1,0:T(8,128)(2,1)} %copy-done.4, ...), custom_call_target="tpu_custom_call", output_to_operand_aliasing={{0}: (14, {}), {1}: (15, {}), {2}: (16, {}), {3}: (17, {}),... | custom-call | flops 5637144576 | bytes 20971520 | tf_op jit(solution)/shard_map/expert_pair/pallas_call | solution.py:213
  145.5 10.2 %fusion.26 = f32[2,2048,512]{2,1,0:T(8,128)} fusion(bf16[2,768,2048]{2,1,0:T(8,128)(2,1)} %get-tuple-element.64, bf16[2,768,512]{2,1,0:T(8,128)(2,1)} %get-tuple-element.66), kind=kOutput, calls=%fused_computation.57 | convolution fusion | flops 3221225472 | bytes 16252928 | tf_op jit(solution)/shard_map/dot_general | solution.py:255
  157.1 5.8 %fusion.25 = f32[2,2048,512]{2,1,0:T(8,128)} fusion(bf16[2,768,2048]{2,1,0:T(8,128)(2,1)S(1)} %copy-done, bf16[2,768,512]{2,1,0:T(8,128)(2,1)S(1)} %copy-done.2), kind=kOutput, calls=%fused_computation.56 | convolution fusion | flops 3221225472 | bytes 16252928 | tf_op jit(solution)/shard_map/dot_general | solution.py:255
  164.6 6.8 %collective-permute-done.7 = bf16[2,264,512]{2,1,0:T(8,128)(2,1)S(1)} collective-permute-done((bf16[2,264,512]{2,1,0:T(8,128)(2,1)S(1)}, bf16[2,264,512]{2,1,0:T(8,128)(2,1)S(1)}, u32[]{:S(2)}, u32[]{:S(2)}) %collective-permute-start.7) | collective-permute-done | bytes 540704 | tf_op jit(solution)/shard_map/ppermute | solution.py:18
  174.6 8.4 %collective-permute-done.23 = bf16[2,264,512]{2,1,0:T(8,128)(2,1)S(1)} collective-permute-done((bf16[2,264,512]{2,1,0:T(8,128)(2,1)S(1)}, bf16[2,264,512]{2,1,0:T(8,128)(2,1)S(1)}, u32[]{:S(2)}, u32[]{:S(2)}) %collective-permute-start.23) | collective-permute-done | bytes 540704 | tf_op jit(solution)/shard_map/ppermute | solution.py:18
  183.8 10.8 %collective-permute-done.26 = bf16[2,264,512]{2,1,0:T(8,128)(2,1)S(1)} collective-permute-done((bf16[2,264,512]{2,1,0:T(8,128)(2,1)S(1)}, bf16[2,264,512]{2,1,0:T(8,128)(2,1)S(1)}, u32[]{:S(2)}, u32[]{:S(2)}) %collective-permute-start.26) | collective-permute-done | bytes 540704 | tf_op jit(solution)/shard_map/ppermute | solution.py:18
  195.4 10.0 %collective-permute-done.40 = bf16[2,264,512]{2,1,0:T(8,128)(2,1)S(1)} collective-permute-done((bf16[2,264,512]{2,1,0:T(8,128)(2,1)S(1)}, bf16[2,264,512]{2,1,0:T(8,128)(2,1)S(1)}, u32[]{:S(2)}, u32[]{:S(2)}) %collective-permute-start.40) | collective-permute-done | bytes 540704 | tf_op jit(solution)/shard_map/ppermute | solution.py:18
  206.3 5.3 %collective-permute-start.28 = (bf16[264,512]{1,0:T(8,128)(2,1)S(1)}, bf16[264,512]{1,0:T(8,128)(2,1)S(1)}, u32[]{:S(2)}, u32[]{:S(2)}) collective-permute-start(bf16[264,512]{1,0:T(8,128)(2,1)S(1)} %fusion.11), channel_id=1, source_target_pairs={{0,16},{4,20},{24,8},{28,12},{1,17},{5,21},{25,9},{29,13},{2,18},{... | collective-permute-start | bytes 811016 | tf_op jit(solution)/shard_map/ppermute | solution.py:300
  215.0 4.1 %collective-permute-start.43 = (bf16[264,512]{1,0:T(8,128)(2,1)S(1)}, bf16[264,512]{1,0:T(8,128)(2,1)S(1)}, u32[]{:S(2)}, u32[]{:S(2)}) collective-permute-start(bf16[264,512]{1,0:T(8,128)(2,1)S(1)} %fusion.9), channel_id=1, source_target_pairs={{0,24},{4,28},{24,0},{28,4},{1,25},{5,29},{25,1},{29,5},{2,26},{6,... | collective-permute-start | bytes 811016 | tf_op jit(solution)/shard_map/ppermute | solution.py:300
  219.1 5.8 %fusion.27 = f32[2,512,2048]{2,1,0:T(8,128)} fusion(bf16[2,768,512]{2,1,0:T(8,128)(2,1)S(1)} %copy-done.1, bf16[2,768,2048]{2,1,0:T(8,128)(2,1)S(1)} %bitcast.71), kind=kOutput, calls=%fused_computation.58 | convolution fusion | flops 3221225472 | bytes 16252928 | tf_op jit(solution)/shard_map/dot_general | solution.py:255
  225.0 10.6 %collective-permute-done.42 = bf16[264,512]{1,0:T(8,128)(2,1)S(1)} collective-permute-done((bf16[264,512]{1,0:T(8,128)(2,1)S(1)}, bf16[264,512]{1,0:T(8,128)(2,1)S(1)}, u32[]{:S(2)}, u32[]{:S(2)}) %collective-permute-start.42) | collective-permute-done | bytes 270368 | tf_op jit(solution)/shard_map/ppermute | solution.py:300
  (163 shorter events, 37.9 us)
Async XLA Ops:
  8.8 29.4 %collective-permute-start = (bf16[264,2048]{1,0:T(8,128)(2,1)S(1)}, bf16[264,2048]{1,0:T(8,128)(2,1)}, u32[]{:S(2)}, u32[]{:S(2)}) collective-permute-start(bf16[264,2048]{1,0:T(8,128)(2,1)S(1)} %pad_maximum_fusion), channel_id=1, source_target_pairs={{0,4},{4,0},{8,12},{12,8},{16,20},{20,16},{24,28},{28,24},{1,5},{5... | collective-permute-start | bytes 3244040 | tf_op jit(solution)/shard_map/ppermute | solution.py:18
  38.2 21.1 %collective-permute-start.18 = (bf16[136,2048]{1,0:T(8,128)(2,1)S(1)}, bf16[136,2048]{1,0:T(8,128)(2,1)S(1)}, u32[]{:S(2)}, u32[]{:S(2)}) collective-permute-start(bf16[136,2048]{1,0:T(8,128)(2,1)S(1)} %broadcast_select_fusion.1.refs_4_), channel_id=1, source_target_pairs={{0,4},{4,0},{8,12},{12,8},{16,20},{20,16},{24,28},{28,24},{1,5},{5... | collective-permute-start | bytes 1671176 | tf_op jit(solution)/shard_map/ppermute | solution.py:18
  39.8 19.5 %collective-permute-start.31 = (bf16[136,2048]{1,0:T(8,128)(2,1)S(1)}, bf16[136,2048]{1,0:T(8,128)(2,1)S(1)}, u32[]{:S(2)}, u32[]{:S(2)}) collective-permute-start(bf16[136,2048]{1,0:T(8,128)(2,1)S(1)} %collective-permute-done.30), channel_id=1, source_target_pairs={{8,0},{12,4},{16,24},{20,28},{9,1},{13,5},{17,25},{21,29},{10,2},{... | collective-permute-start | bytes 1671176 | tf_op jit(solution)/shard_map/ppermute | solution.py:300
  60.0 20.5 %collective-permute-start.19 = (bf16[136,2048]{1,0:T(8,128)(2,1)S(1)}, bf16[136,2048]{1,0:T(8,128)(2,1)S(1)}, u32[]{:S(2)}, u32[]{:S(2)}) collective-permute-start(bf16[136,2048]{1,0:T(8,128)(2,1)S(1)} %collective-permute-done.18.refs_8_), channel_id=1, source_target_pairs={{0,2},{1,3},{2,0},{3,1},{4,6},{5,7},{6,4},{7,5},{8,10},{9,11},{10,... | collective-permute-start | bytes 1671176 | tf_op jit(solution)/shard_map/ppermute | solution.py:18
  61.2 19.3 %collective-permute-start.17 = (bf16[136,2048]{1,0:T(8,128)(2,1)S(1)}, bf16[136,2048]{1,0:T(8,128)(2,1)S(1)}, u32[]{:S(2)}, u32[]{:S(2)}) collective-permute-start(bf16[136,2048]{1,0:T(8,128)(2,1)S(1)} %collective-permute-done.15.refs_5_), channel_id=1, source_target_pairs={{0,1},{1,0},{2,3},{3,2},{4,5},{5,4},{6,7},{7,6},{8,9},{9,8},{10,11... | collective-permute-start | bytes 1671176 | tf_op jit(solution)/shard_map/ppermute | solution.py:18
  69.1 35.8 %collective-permute-start.32 = (bf16[136,2048]{1,0:T(8,128)(2,1)S(1)}, bf16[136,2048]{1,0:T(8,128)(2,1)S(1)}, u32[]{:S(2)}, u32[]{:S(2)}) collective-permute-start(bf16[136,2048]{1,0:T(8,128)(2,1)S(1)} %broadcast_select_fusion.refs_0_), channel_id=1, source_target_pairs={{0,2},{1,3},{2,0},{3,1},{4,6},{5,7},{6,4},{7,5},{8,10},{9,11},{10,... | collective-permute-start | bytes 1671176 | tf_op jit(solution)/shard_map/ppermute | solution.py:18
  70.7 32.5 %collective-permute-start.20 = (bf16[136,2048]{1,0:T(8,128)(2,1)S(1)}, bf16[136,2048]{1,0:T(8,128)(2,1)S(1)}, u32[]{:S(2)}, u32[]{:S(2)}) collective-permute-start(bf16[136,2048]{1,0:T(8,128)(2,1)S(1)} %collective-permute-done.18.refs_8_), channel_id=1, source_target_pairs={{0,1},{1,0},{2,3},{3,2},{4,5},{5,4},{6,7},{7,6},{8,9},{9,8},{10,11... | collective-permute-start | bytes 1671176 | tf_op jit(solution)/shard_map/ppermute | solution.py:18
  80.5 22.7 %collective-permute-start.12 = (bf16[136,2048]{1,0:T(8,128)(2,1)S(1)}, bf16[136,2048]{1,0:T(8,128)(2,1)S(1)}, u32[]{:S(2)}, u32[]{:S(2)}) collective-permute-start(bf16[136,2048]{1,0:T(8,128)(2,1)S(1)} %collective-permute-done.10.refs_1_), channel_id=1, source_target_pairs={{0,1},{1,0},{2,3},{3,2},{4,5},{5,4},{6,7},{7,6},{8,9},{9,8},{10,11... | collective-permute-start | bytes 1671176 | tf_op jit(solution)/shard_map/ppermute | solution.py:18
  80.6 24.9 %collective-permute-start.21 = (bf16[136,2048]{1,0:T(8,128)(2,1)S(1)}, bf16[136,2048]{1,0:T(8,128)(2,1)}, u32[]{:S(2)}, u32[]{:S(2)}) collective-permute-start(bf16[136,2048]{1,0:T(8,128)(2,1)S(1)} %collective-permute-done.19.refs_9_), channel_id=1, source_target_pairs={{0,1},{1,0},{2,3},{3,2},{4,5},{5,4},{6,7},{7,6},{8,9},{9,8},{10,11... | collective-permute-start | bytes 1671176 | tf_op jit(solution)/shard_map/ppermute | solution.py:18
  81.8 23.8 %collective-permute-start.36 = (bf16[136,2048]{1,0:T(8,128)(2,1)S(1)}, bf16[136,2048]{1,0:T(8,128)(2,1)}, u32[]{:S(2)}, u32[]{:S(2)}) collective-permute-start(bf16[136,2048]{1,0:T(8,128)(2,1)S(1)} %collective-permute-done.35.refs_4_), channel_id=1, source_target_pairs={{0,2},{1,3},{2,0},{3,1},{4,6},{5,7},{6,4},{7,5},{8,10},{9,11},{10,... | collective-permute-start | bytes 1671176 | tf_op jit(solution)/shard_map/ppermute | solution.py:18
  103.2 22.9 %collective-permute-start.33 = (bf16[136,2048]{1,0:T(8,128)(2,1)S(1)}, bf16[136,2048]{1,0:T(8,128)(2,1)S(1)}, u32[]{:S(2)}, u32[]{:S(2)}) collective-permute-start(bf16[136,2048]{1,0:T(8,128)(2,1)S(1)} %broadcast_select_fusion.refs_0_), channel_id=1, source_target_pairs={{0,1},{1,0},{2,3},{3,2},{4,5},{5,4},{6,7},{7,6},{8,9},{9,8},{10,11... | collective-permute-start | bytes 1671176 | tf_op jit(solution)/shard_map/ppermute | solution.py:18
  104.9 50.8 %collective-permute-start.6 = (bf16[3,2,264,512]{3,2,1,0:T(8,128)(2,1)}, bf16[3,2,264,512]{3,2,1,0:T(8,128)(2,1)S(1)}, u32[]{:S(2)}, u32[]{:S(2)}) collective-permute-start(bf16[3,2,264,512]{3,2,1,0:T(8,128)(2,1)} %get-tuple-element.39), channel_id=1, source_target_pairs={{0,1},{1,0},{2,3},{3,2},{4,5},{5,4},{6,7},{7,6},{8,9},{9,8},{10,11... | collective-permute-start | bytes 4866056 | tf_op jit(solution)/shard_map/ppermute | solution.py:18
  104.9 21.4 %collective-permute-start.37 = (bf16[136,2048]{1,0:T(8,128)(2,1)S(1)}, bf16[136,2048]{1,0:T(8,128)(2,1)S(1)}, u32[]{:S(2)}, u32[]{:S(2)}) collective-permute-start(bf16[136,2048]{1,0:T(8,128)(2,1)S(1)} %collective-permute-done.35.refs_4_), channel_id=1, source_target_pairs={{0,1},{1,0},{2,3},{3,2},{4,5},{5,4},{6,7},{7,6},{8,9},{9,8},{10,11... | collective-permute-start | bytes 1671176 | tf_op jit(solution)/shard_map/ppermute | solution.py:18
  105.5 20.9 %collective-permute-start.34 = (bf16[136,2048]{1,0:T(8,128)(2,1)S(1)}, bf16[136,2048]{1,0:T(8,128)(2,1)S(1)}, u32[]{:S(2)}, u32[]{:S(2)}) collective-permute-start(bf16[136,2048]{1,0:T(8,128)(2,1)S(1)} %collective-permute-done.32.refs_1_), channel_id=1, source_target_pairs={{0,1},{1,0},{2,3},{3,2},{4,5},{5,4},{6,7},{7,6},{8,9},{9,8},{10,11... | collective-permute-start | bytes 1671176 | tf_op jit(solution)/shard_map/ppermute | solution.py:18
  105.6 20.8 %collective-permute-start.38 = (bf16[136,2048]{1,0:T(8,128)(2,1)}, bf16[136,2048]{1,0:T(8,128)(2,1)S(1)}, u32[]{:S(2)}, u32[]{:S(2)}) collective-permute-start(bf16[136,2048]{1,0:T(8,128)(2,1)} %collective-permute-done.36.refs_5_), channel_id=1, source_target_pairs={{0,1},{1,0},{2,3},{3,2},{4,5},{5,4},{6,7},{7,6},{8,9},{9,8},{10,11... | collective-permute-start | bytes 1671176 | tf_op jit(solution)/shard_map/ppermute | solution.py:18
  126.1 36.8 %collective-permute-start.22 = (bf16[3,2,264,512]{3,2,1,0:T(8,128)(2,1)}, bf16[3,2,264,512]{3,2,1,0:T(8,128)(2,1)S(1)}, u32[]{:S(2)}, u32[]{:S(2)}) collective-permute-start(bf16[3,2,264,512]{3,2,1,0:T(8,128)(2,1)} %get-tuple-element.50), channel_id=1, source_target_pairs={{0,1},{1,0},{2,3},{3,2},{4,5},{5,4},{6,7},{7,6},{8,9},{9,8},{10,11... | collective-permute-start | bytes 4866056 | tf_op jit(solution)/shard_map/ppermute | solution.py:18
  145.1 27.6 %collective-permute-start.39 = (bf16[2,2,264,512]{3,2,1,0:T(8,128)(2,1)}, bf16[2,2,264,512]{3,2,1,0:T(8,128)(2,1)S(1)}, u32[]{:S(2)}, u32[]{:S(2)}) collective-permute-start(bf16[2,2,264,512]{3,2,1,0:T(8,128)(2,1)} %get-tuple-element.61), channel_id=1, source_target_pairs={{0,1},{1,0},{2,3},{3,2},{4,5},{5,4},{6,7},{7,6},{8,9},{9,8},{10,11... | collective-permute-start | bytes 3244040 | tf_op jit(solution)/shard_map/ppermute | solution.py:18
  163.4 19.6 %collective-permute-start.23 = (bf16[2,264,512]{2,1,0:T(8,128)(2,1)S(1)}, bf16[2,264,512]{2,1,0:T(8,128)(2,1)S(1)}, u32[]{:S(2)}, u32[]{:S(2)}) collective-permute-start(bf16[2,264,512]{2,1,0:T(8,128)(2,1)S(1)} %get-tuple-element.51), channel_id=1, source_target_pairs={{0,4},{4,0},{8,12},{12,8},{16,20},{20,16},{24,28},{28,24},{1,5},{5... | collective-permute-start | bytes 1622024 | tf_op jit(solution)/shard_map/ppermute | solution.py:18
  171.6 43.4 %collective-permute-start.8 = (bf16[264,512]{1,0:T(8,128)(2,1)S(1)}, bf16[264,512]{1,0:T(8,128)(2,1)S(1)}, u32[]{:S(2)}, u32[]{:S(2)}) collective-permute-start(bf16[264,512]{1,0:T(8,128)(2,1)S(1)} %fusion.21), channel_id=1, source_target_pairs={{0,2},{1,3},{2,0},{3,1},{4,6},{5,7},{6,4},{7,5},{8,10},{9,11},{10,... | collective-permute-start | bytes 811016 | tf_op jit(solution)/shard_map/ppermute | solution.py:18
  172.2 22.4 %collective-permute-start.26 = (bf16[2,264,512]{2,1,0:T(8,128)(2,1)S(1)}, bf16[2,264,512]{2,1,0:T(8,128)(2,1)S(1)}, u32[]{:S(2)}, u32[]{:S(2)}) collective-permute-start(bf16[2,264,512]{2,1,0:T(8,128)(2,1)S(1)} %get-tuple-element.53), channel_id=1, source_target_pairs={{0,4},{4,0},{8,12},{12,8},{16,20},{20,16},{24,28},{28,24},{1,5},{5... | collective-permute-start | bytes 1622024 | tf_op jit(solution)/shard_map/ppermute | solution.py:18
  173.0 32.4 %collective-permute-start.40 = (bf16[2,264,512]{2,1,0:T(8,128)(2,1)S(1)}, bf16[2,264,512]{2,1,0:T(8,128)(2,1)S(1)}, u32[]{:S(2)}, u32[]{:S(2)}) collective-permute-start(bf16[2,264,512]{2,1,0:T(8,128)(2,1)S(1)} %get-tuple-element.63), channel_id=1, source_target_pairs={{0,4},{4,0},{8,12},{12,8},{16,20},{20,16},{24,28},{28,24},{1,5},{5... | collective-permute-start | bytes 1622024 | tf_op jit(solution)/shard_map/ppermute | solution.py:18
  183.2 29.1 %collective-permute-start.24 = (bf16[264,512]{1,0:T(8,128)(2,1)S(1)}, bf16[264,512]{1,0:T(8,128)(2,1)S(1)}, u32[]{:S(2)}, u32[]{:S(2)}) collective-permute-start(bf16[264,512]{1,0:T(8,128)(2,1)S(1)} %fusion.22), channel_id=1, source_target_pairs={{0,2},{1,3},{2,0},{3,1},{4,6},{5,7},{6,4},{7,5},{8,10},{9,11},{10,... | collective-permute-start | bytes 811016 | tf_op jit(solution)/shard_map/ppermute | solution.py:18
  213.7 21.9 %collective-permute-start.42 = (bf16[264,512]{1,0:T(8,128)(2,1)S(1)}, bf16[264,512]{1,0:T(8,128)(2,1)S(1)}, u32[]{:S(2)}, u32[]{:S(2)}) collective-permute-start(bf16[264,512]{1,0:T(8,128)(2,1)S(1)} %fusion.9), channel_id=1, source_target_pairs={{8,24},{12,28},{16,0},{20,4},{9,25},{13,29},{17,1},{21,5},{10,26},... | collective-permute-start | bytes 811016 | tf_op jit(solution)/shard_map/ppermute | solution.py:300
  215.0 20.6 %collective-permute-start.43 = (bf16[264,512]{1,0:T(8,128)(2,1)S(1)}, bf16[264,512]{1,0:T(8,128)(2,1)S(1)}, u32[]{:S(2)}, u32[]{:S(2)}) collective-permute-start(bf16[264,512]{1,0:T(8,128)(2,1)S(1)} %fusion.9), channel_id=1, source_target_pairs={{0,24},{4,28},{24,0},{28,4},{1,25},{5,29},{25,1},{29,5},{2,26},{6,... | collective-permute-start | bytes 811016 | tf_op jit(solution)/shard_map/ppermute | solution.py:300
  (53 other events, 968.1 us)
